TPU v7x, 512 devices: a whole 4x4x16 slice. The times are simulated.
512 devices in a mesh: sp: 32 (over z, core), tp: 16 (over y, x).
Axes of the slice: x: 4, y: 4, z: 16, core: 2. Of those that a mesh axis runs over, the one named last changes fastest.
Arguments:
- pool_in: bfloat16 [512, 12288], P('tp', 'sp'), may hold values from -8 to 8
- doc_ids: int32 [12288], P('sp'), may hold values from 0 to 15, never falling along the last dimension, each value on 1 to 1536 neighbouring positions
- pool_map: bfloat16 [8, 64, 64], replicated, may hold values from -0.75 to 0.75
- pool_scale: float32 [512], replicated, may hold values from 0.1 to 1.9
- w_out: bfloat16 [512, 2048], P(None, 'tp'), may hold values from -0.25 to 0.25
- gate_logit: bfloat16 [12288, 2048], P('sp', 'tp'), may hold values from -8 to 8
- residual: bfloat16 [12288, 2048], P('sp', 'tp'), may hold values from -4 to 4
- first_gain: float32 [2048], P('tp'), may hold values from 0.1 to 1.9
- first_bias: float32 [2048], P('tp'), may hold values from -1.5 to 1.5
- routes: int32 [12288, 2], P('sp'), may hold values from 0 to 31, all different within a row; in each aligned block of 384 rows (0 to 383, 384 to 767, ...) at most 48 rows name the same one
- route_weight: float32 [12288, 2], P('sp'), may hold values from 0.25 to 1
- w_gate: bfloat16 [32, 2048, 1024], P('sp', None, 'tp'), may hold values from -0.125 to 0.125
- w_up: bfloat16 [32, 2048, 1024], P('sp', None, 'tp'), may hold values from -0.125 to 0.125
- w_down: bfloat16 [32, 1024, 2048], P('sp', None, 'tp'), may hold values from -0.375 to 0.375
- second_gain: float32 [2048], P('tp'), may hold values from 0.1 to 1.9
- second_bias: float32 [2048], P('tp'), may hold values from -1.5 to 1.5
Outputs:
- layer_out: bfloat16 [12288, 2048], P('sp', 'tp')
Inputs may be any that keep to these rules, and one draw needn't show every extreme that they name: `doc_ids`: never falling; each document spans 1 to 1536 positions. `routes`: each row names 2 different experts; in each aligned block of 384 rows (the rows of one index of sp) no expert is named by more than 48 rows, a bound that some block reaches.
All inputs are finite; a program needn't handle non-finite values.
Results may differ from a plain program's by a relative error of at most 0.008.
Values may be sent and summed in bfloat16 or wider, within the bound.
A program may use at most 64 MiB of HBM per device.

v0:
```python
import functools

import jax
import jax.numpy as jnp
from jax import lax
from jax.sharding import Mesh
from jax.sharding import PartitionSpec as P

GROUP_W = 64
TP = ("tp_0", "tp_1")


EPS = 1e-05
ALPHA = 8.0**0.25
halo_len = 16


def shifted(shard, axis, by):
    size = lax.axis_size(axis)
    pairs = [(i, i + by) for i in range(size) if 0 <= i + by < size]
    return lax.ppermute(shard, axis, pairs)


def copy_for_each(shard, axis):
    copies = jnp.broadcast_to(shard, (lax.axis_size(axis), *shard.shape))
    return lax.all_to_all(copies, axis, split_axis=0, concat_axis=0, tiled=True)


def all_in_one(shard, axis):
    leaves = jax.tree.leaves(shard)
    turns = sorted(range(len(leaves)), key=lambda k: -leaves[k].size)
    width = (1, *leaves[turns[0]].shape)[-1]
    lines = [
        jnp.pad(leaves[k].reshape(-1), (0, -leaves[k].size % width)).reshape(-1, width)
        for k in turns
    ]
    both, at, found = (copy_for_each(jnp.concatenate(lines), axis), 0, {})
    for k, line in zip(turns, lines):
        piece = both[:, at : at + len(line)].reshape(len(both), -1)
        found[k] = piece[:, : leaves[k].size].reshape(-1, *leaves[k].shape)
        at += len(line)
    numbers = iter(range(len(leaves)))
    return jax.tree.map(lambda _: found[next(numbers)], shard)


def combined_pairwise(pieces, combine):
    while len(jax.tree.leaves(pieces)[0]) > 1:
        pieces = jax.vmap(combine)(
            *(jax.tree.map(lambda part: part[side::2], pieces) for side in (0, 1))
        )
    return jax.tree.map(lambda part: part[0], pieces)


def carried_in(shard, axis, combine, identity):
    size, place = (lax.axis_size(axis), lax.axis_index(axis))
    passed = jnp.arange(size) < place

    def kept(part, zero, own):
        part = jnp.where(
            passed.reshape(-1, *(1 for _ in own.shape)), part, jnp.asarray(zero, own.dtype)
        )
        return part

    pieces = all_in_one(shard, axis)
    return combined_pairwise(jax.tree.map(kept, pieces, identity, shard), combine)


def in_order(pieces, dim):
    pieces = jnp.moveaxis(pieces, 0, dim)
    dims = pieces.shape
    return pieces.reshape(*dims[:dim], dims[dim] * dims[dim + 1], *dims[dim + 2 :])


def collect(shard, axis, dim):
    pieces = copy_for_each(shard, axis)
    return in_order(pieces, dim)


def over_axes(shard, axes):
    return functools.reduce(lax.psum, axes, shard)


def gathered_by_axis(shard, axes, dim):
    out = shard
    for number in range(len(axes) - 1, -1, -1):
        out = lax.all_gather(out, axes[number], axis=dim, tiled=True)
    return out


def carry_join(earlier, later):
    keeping = 1.0 - later[2]
    return (
        later[0] + keeping * earlier[0],
        later[1] + keeping * earlier[1],
        jnp.maximum(earlier[2], later[2]),
    )


def apply_norm(row_data, totals, gain_vec, bias_vec, features):
    row_mean = totals[0][:, None] / features
    row_var = totals[1][:, None] / features - row_mean * row_mean
    return (row_data - row_mean) * lax.rsqrt(row_var + EPS) * gain_vec + bias_vec


def pool_scales(pool_in, doc_ids):
    channels_dev, positions = pool_in.shape
    edge_block = jnp.concatenate(
        [
            pool_in[:, positions - halo_len :],
            doc_ids[None, positions - halo_len :].astype(jnp.bfloat16),
        ],
        axis=0,
    )
    previous = shifted(edge_block, "sp", 1)
    prior_ids = jnp.where(
        lax.axis_index("sp") == 0, -1.0, previous[channels_dev].astype(jnp.float32)
    )
    ids_ext = jnp.concatenate([prior_ids, doc_ids.astype(jnp.float32)])
    inputs_ext = jnp.concatenate([previous[:channels_dev], pool_in], axis=1).astype(jnp.float32)
    length = positions + halo_len
    opening = jnp.concatenate([jnp.zeros((1,), bool), ids_ext[1:] != ids_ext[:-1]])
    places = jnp.arange(length, dtype=jnp.int32)
    doc_start = lax.cummax(jnp.where(opening, places, 0), axis=0)
    prefix = jnp.concatenate(
        [jnp.zeros((channels_dev, 1), jnp.float32), jnp.cumsum(inputs_ext, axis=1)], axis=1
    )
    start_here = doc_start[halo_len:]
    upper_at = places[halo_len:] + 1
    at_start = jnp.take(prefix, start_here, axis=1)
    current = prefix[:, halo_len + 1 :]
    group_id = (
        lax.axis_index(TP) * channels_dev + jnp.arange(channels_dev, dtype=jnp.int32)
    ) // GROUP_W
    doc_mask = (group_id % 2 == 1)[:, None]
    window = jnp.left_shift(2, group_id // 2 % 4)[:, None]
    lagged = jnp.zeros((channels_dev, positions), jnp.float32)
    for octave in range(4):
        window_len = 2 << octave
        begin = halo_len + 1 - window_len
        lagged = lagged + jnp.where(window == window_len, prefix[:, begin : begin + positions], 0.0)
    lower_at = jnp.maximum(upper_at[None, :] - window, start_here[None, :])
    win_sum = current - jnp.where(
        start_here[None, :] > upper_at[None, :] - window, at_start, lagged
    )
    win_count = (upper_at[None, :] - lower_at).astype(jnp.float32)
    opened = start_here >= halo_len
    local_sum = current - jnp.where(opened[None, :], at_start, prefix[:, halo_len : halo_len + 1])
    local_count = (upper_at - jnp.maximum(start_here, halo_len)).astype(jnp.float32)
    last_start = doc_start[length - 1]
    last_base = jnp.where(
        last_start >= halo_len,
        lax.dynamic_slice_in_dim(prefix, last_start, 1, 1)[:, 0],
        prefix[:, halo_len],
    )
    summary = (
        prefix[:, length] - last_base,
        (length - jnp.maximum(last_start, halo_len)).astype(jnp.float32),
        (last_start >= halo_len).astype(jnp.float32),
    )
    nothing = (jnp.zeros((channels_dev,), jnp.float32), jnp.float32(0.0), jnp.float32(0.0))
    carried = carried_in(summary, "sp", carry_join, nothing)
    doc_sum = local_sum + jnp.where(opened[None, :], 0.0, carried[0][:, None])
    doc_count = local_count + jnp.where(opened, 0.0, carried[1])
    pooled = (
        jnp.where(doc_mask, doc_sum / doc_count[None, :], win_sum / win_count)
        - inputs_ext[:, halo_len:]
    )
    return pooled.astype(jnp.bfloat16)


def body(
    pool_in,
    doc_ids,
    pool_map,
    pool_scale,
    w_out,
    gate_logit,
    residual,
    first_gain,
    first_bias,
    routes,
    route_weight,
    w_gate,
    w_up,
    w_down,
    second_gain,
    second_bias,
):
    pooled = pool_scales(pool_in, doc_ids)
    positions = pool_in.shape[1]
    features = residual.shape[1] * lax.axis_size(TP)
    gathered = collect(pooled, TP, 0)
    group_count = gathered.shape[0] // GROUP_W
    grouped = jnp.einsum(
        "gct,gcd->tgd",
        gathered.reshape(group_count, GROUP_W, positions),
        pool_map,
        preferred_element_type=jnp.float32,
    )
    mapped = (grouped.reshape(positions, group_count * GROUP_W) * pool_scale).astype(jnp.bfloat16)
    mixer_out = jnp.dot(mapped, w_out, preferred_element_type=jnp.float32) * jax.nn.sigmoid(
        gate_logit.astype(jnp.float32)
    )
    mixed_rows = ALPHA * residual.astype(jnp.float32) + mixer_out
    first_totals = (
        over_axes(jnp.sum(mixed_rows, axis=1), TP),
        over_axes(jnp.sum(mixed_rows * mixed_rows, axis=1), TP),
    )
    normed = apply_norm(mixed_rows, first_totals, first_gain, first_bias, features).astype(
        jnp.bfloat16
    )
    experts = lax.axis_size("sp")
    pairs = routes.shape[1]
    slots_per = 2 * positions * pairs // experts
    flat_routes = routes.reshape(-1)
    one_hot = (flat_routes[:, None] == jnp.arange(experts, dtype=jnp.int32)[None, :]).astype(
        jnp.int32
    )
    slot_rank = jnp.sum((jnp.cumsum(one_hot, axis=0, dtype=jnp.int32) - 1) * one_hot, axis=1)
    slot_ids = flat_routes * slots_per + slot_rank
    token_of = jnp.arange(flat_routes.shape[0], dtype=jnp.int32) // pairs
    outgoing = (
        jnp.zeros((experts * slots_per, normed.shape[1]), jnp.bfloat16)
        .at[slot_ids]
        .set(normed[token_of])
    )
    arrived = lax.all_to_all(outgoing, "sp", split_axis=0, concat_axis=0, tiled=True)
    inputs = lax.all_gather(arrived, TP, axis=1, tiled=True)
    gate_part = jnp.dot(inputs, w_gate[0], preferred_element_type=jnp.float32)
    up_part = jnp.dot(inputs, w_up[0], preferred_element_type=jnp.float32)
    hidden = (jax.nn.silu(gate_part) * up_part).astype(jnp.bfloat16)
    down_part = w_down[0]
    result = jnp.dot(gathered_by_axis(hidden, TP, 1), down_part, preferred_element_type=jnp.float32)
    returned = lax.all_to_all(
        result.astype(jnp.bfloat16), "sp", split_axis=0, concat_axis=0, tiled=True
    )
    picked = returned[slot_ids].astype(jnp.float32).reshape(positions, pairs, returned.shape[1])
    moe_sum = jnp.sum(picked * route_weight[:, :, None], axis=1)
    final_rows = ALPHA * normed.astype(jnp.float32) + moe_sum
    second_totals = (
        over_axes(jnp.sum(final_rows, axis=1), TP),
        over_axes(jnp.sum(final_rows * final_rows, axis=1), TP),
    )
    return apply_norm(final_rows, second_totals, second_gain, second_bias, features).astype(
        jnp.bfloat16
    )


def solution(mesh):
    finer = Mesh(mesh.devices.reshape(mesh.shape["sp"], 4, 4), ("sp", "tp_0", "tp_1"))
    in_specs = (
        P(TP, "sp"),
        P("sp"),
        P(),
        P(),
        P(None, TP),
        P("sp", TP),
        P("sp", TP),
        P(TP),
        P(TP),
        P("sp", None),
        P("sp", None),
        P("sp", None, TP),
        P("sp", None, TP),
        P("sp", None, TP),
        P(TP),
        P(TP),
    )
    out_specs = P("sp", TP)
    return jax.shard_map(body, mesh=finer, in_specs=in_specs, out_specs=out_specs, check_vma=False)
```

profile of v0, /device:TPU:1, one launch (start us, length us, event | category | flops | bytes accessed | tf_op | source)
XLA Modules:
  0.0 342.4 jit_solution(7189433196798893878)
XLA Ops:
  6.6 0.8 fusion.42
  7.4 0.8 slice.196
  8.2 4.9 %collective-permute-start = (bf16[33,16]{1,0:T(8,128)(2,1)S(1)}, bf16[33,16]{1,0:T(8,128)(2,1)S(1)}, u32[]{:S(2)}, u32[]{:S(2)}) collective-permute-start(bf16[33,16]{1,0:T(8,128)(2,1)S(1)} %pad_maximum_fusion), channel_id=1, source_target_pairs={{0,16},{16,32},{32,48},{48,64},{64,80},{80,96},{96,112},{112,128},... | collective-permute-start | bytes 3176 | tf_op jit(solution)/shard_map/ppermute | solution.py:21
  13.2 0.8 copy.179
  14.1 0.7 broadcast_multiply_fusion
  15.0 1.7 reduce-window.29
  21.2 0.8 maximum_convert_fusion
  22.0 1.2 reduce-window.21
  25.2 14.3 %all-to-all-start = ((f32[32,3,32]{2,1,0:T(4,128)}), f32[32,3,32]{2,1,0:T(4,128)S(1)}, u32[]{:S(2)}, u32[]{:S(2)}) async-start(f32[32,3,32]{2,1,0:T(4,128)} %broadcast_in_dim.171), calls=%async_computation | async-start | bytes 131072 | tf_op jit(solution)/shard_map/all_to_all | solution.py:26
  39.5 1.1 gather_fusion
  40.7 11.7 %all-to-all-done = f32[32,3,32]{2,1,0:T(4,128)S(1)} async-done(((f32[32,3,32]{2,1,0:T(4,128)}), f32[32,3,32]{2,1,0:T(4,128)S(1)}, u32[]{:S(2)}, u32[]{:S(2)}) %all-to-all-start) | async-done | bytes 12320 | tf_op jit(solution)/shard_map/all_to_all | solution.py:26
  58.3 0.8 broadcast_in_dim.182
  59.1 6.8 %all-to-all-start.1 = ((bf16[16,32,384]{2,1,0:T(8,128)(2,1)}), bf16[16,32,384]{2,1,0:T(8,128)(2,1)S(1)}, u32[]{:S(2)}, u32[]{:S(2)}) async-start(bf16[16,32,384]{2,1,0:T(8,128)(2,1)} %broadcast_in_dim.182), calls=%async_computation.1 | async-start | bytes 786432 | tf_op jit(solution)/shard_map/all_to_all | solution.py:26
  66.3 1.0 copy.169
  67.3 1.0 copy.177
  68.8 5.3 %all-to-all-done.1 = bf16[16,32,384]{2,1,0:T(8,128)(2,1)S(1)} async-done(((bf16[16,32,384]{2,1,0:T(8,128)(2,1)}), bf16[16,32,384]{2,1,0:T(8,128)(2,1)S(1)}, u32[]{:S(2)}, u32[]{:S(2)}) %all-to-all-start.1) | async-done | bytes 393248 | tf_op jit(solution)/shard_map/all_to_all | solution.py:26
  74.9 6.8 %all-reduce.8 = (f32[384]{0:T(512)S(1)}, f32[384]{0:T(512)S(1)}) all-reduce(f32[384]{0:T(512)S(1)} %get-tuple-element.8, f32[384]{0:T(512)S(1)} %get-tuple-element.7), channel_id=1, replica_groups=mesh['sp'=32,'tp_0'=4,'tp_1'=4] {'tp_0'}, use_global_device_ids=true, to_apply=%region_8.9 | all-reduce | flops 768 | bytes 6144 | tf_op jit(solution)/shard_map/psum | solution.py:80
  81.8 6.6 %all-reduce.6 = (f32[384]{0:T(512)S(1)}, f32[384]{0:T(512)S(1)}) all-reduce(f32[384]{0:T(512)S(1)} %get-tuple-element.15, f32[384]{0:T(512)S(1)} %get-tuple-element.16), channel_id=1, replica_groups=mesh['sp'=32,'tp_0'=4,'tp_1'=4] {'tp_1'}, use_global_device_ids=true, to_apply=%region_9.10 | all-reduce | flops 768 | bytes 6144 | tf_op jit(solution)/shard_map/psum | solution.py:80
  88.6 7.5 %scatter_custom_fusion = bf16[1536,128]{1,0:T(8,128)(2,1)S(1)} fusion(s32[768]{0:T(1024)S(1)} %fusion.29, bf16[384,128]{1,0:T(8,128)(2,1)S(1)} %copy.182, s32[1024]{0:T(1024)S(1)} %pad_clamp_fusion.1, bf16[]{:T(256)} %constant.151.clone.1), kind=kCustom, calls=%fused_computation.17 | custom fusion | bytes 393218 | tf_op jit(solution)/shard_map/scatter | solution.py:225
  96.1 38.0 %all_to_all.34 = bf16[32,48,128]{2,1,0:T(8,128)(2,1)} all-to-all(bf16[32,48,128]{2,1,0:T(8,128)(2,1)S(1)} %bitcast.97), channel_id=1, replica_groups=mesh['sp'=32,'tp_0'=4,'tp_1'=4] {'sp'}, dimensions={0} | all-to-all | bytes 786432 | tf_op jit(solution)/shard_map/all_to_all | solution.py:227
  134.3 68.3 %all-gather.3.cloned.1.call-done = bf16[1536,2048]{1,0:T(8,128)(2,1)} async-done(((bf16[1536,128]{1,0:T(8,128)(2,1)}), bf16[1536,2048]{1,0:T(8,128)(2,1)}) %all-gather.3.cloned.1.call-update) | async-done | bytes 6291472 | tf_op jit(solution)/shard_map/all_gather | solution.py:228
  202.6 5.0 %fusion.6 = f32[1536,64]{0,1:T(8,128)S(1)} fusion(bf16[1536,2048]{1,0:T(8,128)(2,1)} %all-gather.3.cloned.1.call-done, bf16[1,2048,64]{1,2,0:T(8,128)(2,1)S(1)} %copy-done.2), kind=kOutput, calls=%fused_computation.15 | convolution fusion | flops 402653184 | bytes 6946816 | tf_op jit(solution)/shard_map/dot_general | solution.py:229
  207.6 2.0 fusion
  209.6 12.4 %all_gather.10 = bf16[1536,256]{0,1:T(8,128)(2,1)} all-gather(bf16[1536,64]{0,1:T(8,128)(2,1)S(1)} %fusion), channel_id=1, replica_groups=mesh['sp'=32,'tp_0'=4,'tp_1'=4] {'tp_1'}, dimensions={1}, use_global_device_ids=true | all-gather | bytes 983040 | tf_op jit(solution)/shard_map/all_gather | solution.py:86
  222.1 50.2 %all-gather.5.cloned.1.call-done = bf16[1536,1024]{0,1:T(8,128)(2,1)} async-done(((bf16[1536,256]{0,1:T(8,128)(2,1)}), bf16[1536,1024]{0,1:T(8,128)(2,1)}) %all-gather.5.cloned.1.call-update) | async-done | bytes 3145744 | tf_op jit(solution)/shard_map/all_gather | solution.py:86
  272.2 3.7 %convolution_convert_fusion = bf16[1536,128]{1,0:T(8,128)(2,1)} fusion(bf16[1536,1024]{0,1:T(8,128)(2,1)} %all-gather.5.cloned.1.call-done, bf16[1,1024,128]{2,1,0:T(8,128)(2,1)S(1)} %copy-done), kind=kOutput, calls=%fused_computation.4 | convolution fusion | flops 402849792 | bytes 3801088 | tf_op jit(solution)/shard_map/dot_general | solution.py:233
  275.9 13.2 %all-to-all-start.3 = ((bf16[32,48,128]{2,1,0:T(8,128)(2,1)}), bf16[32,48,128]{2,1,0:T(8,128)(2,1)S(1)}, u32[]{:S(2)}, u32[]{:S(2)}) async-start(bf16[32,48,128]{2,1,0:T(8,128)(2,1)} %bitcast.27), calls=%async_computation.3 | async-start | bytes 786432 | tf_op jit(solution)/shard_map/all_to_all | solution.py:234
  289.3 27.6 %all-to-all-done.3 = bf16[32,48,128]{2,1,0:T(8,128)(2,1)S(1)} async-done(((bf16[32,48,128]{2,1,0:T(8,128)(2,1)}), bf16[32,48,128]{2,1,0:T(8,128)(2,1)S(1)}, u32[]{:S(2)}, u32[]{:S(2)}) %all-to-all-start.3) | async-done | bytes 393248 | tf_op jit(solution)/shard_map/all_to_all | solution.py:234
  316.9 1.9 gather_fusion.1
  319.6 6.7 %all-reduce.7 = (f32[384]{0:T(512)S(1)}, f32[384]{0:T(512)S(1)}) all-reduce(f32[384]{0:T(512)S(1)} %get-tuple-element.6, f32[384]{0:T(512)S(1)} %get-tuple-element.5), channel_id=1, replica_groups=mesh['sp'=32,'tp_0'=4,'tp_1'=4] {'tp_0'}, use_global_device_ids=true, to_apply=%region_19.20 | all-reduce | flops 768 | bytes 6144 | tf_op jit(solution)/shard_map/psum | solution.py:80
  326.2 8.4 %all-reduce.5 = (f32[384]{0:T(512)S(1)}, f32[384]{0:T(512)S(1)}) all-reduce(f32[384]{0:T(512)S(1)} %get-tuple-element.13, f32[384]{0:T(512)S(1)} %get-tuple-element.14), channel_id=1, replica_groups=mesh['sp'=32,'tp_0'=4,'tp_1'=4] {'tp_1'}, use_global_device_ids=true, to_apply=%region_20.21 | all-reduce | flops 768 | bytes 6144 | tf_op jit(solution)/shard_map/psum | solution.py:80
  334.8 0.8 copy.185
  (135 shorter events, 10.9 us)
Async XLA Ops:
  6.5 265.7 %copy-start = (bf16[1,1024,128]{2,1,0:T(8,128)(2,1)S(1)}, bf16[1,1024,128]{2,1,0:T(8,128)(2,1)}, u32[]{:S(2)}) copy-start(bf16[1,1024,128]{2,1,0:T(8,128)(2,1)} %param.29) | copy-start | bytes 786436
  6.5 67.6 %copy-start.3 = (bf16[8,64,64]{2,1,0:T(8,128)(2,1)S(1)}, bf16[8,64,64]{2,1,0:T(8,128)(2,1)}, u32[]{:S(2)}) copy-start(bf16[8,64,64]{2,1,0:T(8,128)(2,1)} %param.18) | copy-start | bytes 196612
  6.5 67.9 %copy-start.7 = (f32[512]{0:T(512)S(1)}, f32[512]{0:T(512)}, u32[]{:S(2)}) copy-start(f32[512]{0:T(512)} %param.19) | copy-start | bytes 6148
  6.5 68.1 %copy-start.11 = (bf16[512,128]{1,0:T(8,128)(2,1)S(1)}, bf16[512,128]{1,0:T(8,128)(2,1)}, u32[]{:S(2)}) copy-start(bf16[512,128]{1,0:T(8,128)(2,1)} %param.20) | copy-start | bytes 393220
  6.5 81.8 %copy-start.5 = (f32[128]{0:T(128)S(1)}, f32[128]{0:T(128)}, u32[]{:S(2)}) copy-start(f32[128]{0:T(128)} %param.23) | copy-start | bytes 1540
  6.5 81.8 %copy-start.4 = (f32[128]{0:T(128)S(1)}, f32[128]{0:T(128)}, u32[]{:S(2)}) copy-start(f32[128]{0:T(128)} %param.24) | copy-start | bytes 1540
  8.2 8.8 %collective-permute-start = (bf16[33,16]{1,0:T(8,128)(2,1)S(1)}, bf16[33,16]{1,0:T(8,128)(2,1)S(1)}, u32[]{:S(2)}, u32[]{:S(2)}) collective-permute-start(bf16[33,16]{1,0:T(8,128)(2,1)S(1)} %pad_maximum_fusion), channel_id=1, source_target_pairs={{0,16},{16,32},{32,48},{48,64},{64,80},{80,96},{96,112},{112,128},... | collective-permute-start | bytes 3176 | tf_op jit(solution)/shard_map/ppermute | solution.py:21
  14.8 187.8 %copy-start.2 = (bf16[1,2048,64]{1,2,0:T(8,128)(2,1)S(1)}, bf16[1,2048,64]{1,2,0:T(8,128)(2,1)}, u32[]{:S(2)}) copy-start(bf16[1,2048,64]{1,2,0:T(8,128)(2,1)} %param.27) | copy-start | bytes 786436
  25.2 27.3 %all-to-all-start = ((f32[32,3,32]{2,1,0:T(4,128)}), f32[32,3,32]{2,1,0:T(4,128)S(1)}, u32[]{:S(2)}, u32[]{:S(2)}) async-start(f32[32,3,32]{2,1,0:T(4,128)} %broadcast_in_dim.171), calls=%async_computation | async-start | bytes 131072 | tf_op jit(solution)/shard_map/all_to_all | solution.py:26
  59.1 15.1 %all-to-all-start.1 = ((bf16[16,32,384]{2,1,0:T(8,128)(2,1)}), bf16[16,32,384]{2,1,0:T(8,128)(2,1)S(1)}, u32[]{:S(2)}, u32[]{:S(2)}) async-start(bf16[16,32,384]{2,1,0:T(8,128)(2,1)} %broadcast_in_dim.182), calls=%async_computation.1 | async-start | bytes 786432 | tf_op jit(solution)/shard_map/all_to_all | solution.py:26
  65.9 136.7 %all-gather.3.cloned.1.call-start = ((), (), s32[]{:S(2)}) async-start(), calls=%async_computation.4 | async-start | bytes 6684672 | tf_op jit(solution)/shard_map/all_gather | solution.py:228
  74.1 133.4 %copy-start.10 = (bf16[1,2048,64]{1,2,0:T(8,128)(2,1)S(1)}, bf16[1,2048,64]{1,2,0:T(8,128)(2,1)}, u32[]{:S(2)}) copy-start(bf16[1,2048,64]{1,2,0:T(8,128)(2,1)} %param.28) | copy-start | bytes 786436
  134.1 138.2 %all-gather.5.cloned.1.call-start = ((), (), s32[]{:S(2)}) async-start(), calls=%async_computation.5 | async-start | bytes 3932160 | tf_op jit(solution)/shard_map/all_gather | solution.py:86
  202.6 5.0 %copy-start.1 = (bf16[1536,2048]{1,0:T(8,128)(2,1)S(1)}, bf16[1536,2048]{1,0:T(8,128)(2,1)}, u32[]{:S(2)}) copy-start(bf16[1536,2048]{1,0:T(8,128)(2,1)} %all-gather.3.cloned.1.call-done) | copy-start | bytes 18874372
  207.6 81.5 %copy-start.6 = (f32[384,2]{0,1:T(2,128)S(1)}, f32[384,2]{0,1:T(2,128)}, u32[]{:S(2)}) copy-start(f32[384,2]{0,1:T(2,128)} %param.26) | copy-start | bytes 9220
  209.6 125.0 %copy-start.8 = (f32[128]{0:T(128)S(1)}, f32[128]{0:T(128)}, u32[]{:S(2)}) copy-start(f32[128]{0:T(128)} %param.31) | copy-start | bytes 1540
  209.6 125.0 %copy-start.9 = (f32[128]{0:T(128)S(1)}, f32[128]{0:T(128)}, u32[]{:S(2)}) copy-start(f32[128]{0:T(128)} %param.30) | copy-start | bytes 1540
  275.9 40.9 %all-to-all-start.3 = ((bf16[32,48,128]{2,1,0:T(8,128)(2,1)}), bf16[32,48,128]{2,1,0:T(8,128)(2,1)S(1)}, u32[]{:S(2)}, u32[]{:S(2)}) async-start(bf16[32,48,128]{2,1,0:T(8,128)(2,1)} %bitcast.27), calls=%async_computation.3 | async-start | bytes 786432 | tf_op jit(solution)/shard_map/all_to_all | solution.py:234
Sparse Core Ops, SparseCore 0:
  134.2 68.3 all-gather.2
  222.2 50.0 all-gather.4
where the time goes:
time: 346 us; the launch traced here: 342 us
  waiting for transfers between devices  163 us (47%)
  blocking collectives  78.8 us (23%)
  starting transfers between devices  39.4 us (11%)
  local copies, waits for them, and re-layouts  22.3 us (6%)
  between operations  19 us (5%)
  matrix products  11.3 us (3%)
  other arithmetic  8.31 us (2%)
    all_gather x1, waiting for transfers between devices, body(): inputs = lax.all_gather(arrived, TP, axis=1, tiled=True)  68.3 us
    all_gather x1, waiting for transfers between devices, gathered_by_axis(): out = lax.all_gather(out, axes[number], axis=dim, tiled=True)  50.2 us
    all_to_all x1, blocking collectives, body(): lax.all_to_all(outgoing, 'sp', split_axis=0, concat_axis=0, tiled=True)  38 us
    psum x4, blocking collectives, over_axes(): return functools.reduce(lax.psum, axes, shard)  28.4 us
    all_to_all x1, waiting for transfers between devices, body(): lax.all_to_all(result.astype(jnp.bfloat16), 'sp', split_axis=0, concat_ax...  27.6 us
    all_to_all x2, starting transfers between devices, copy_for_each(): return lax.all_to_all(copies, axis, split_axis=0, concat_axis=0, tiled=True)  21 us
    all_to_all x2, waiting for transfers between devices, copy_for_each(): return lax.all_to_all(copies, axis, split_axis=0, concat_axis=0, tiled=True)  17 us
    all_to_all x1, starting transfers between devices, body(): lax.all_to_all(result.astype(jnp.bfloat16), 'sp', split_axis=0, concat_ax...  13.2 us
  transfers between devices with their start and end apart: 6, of which 6 were waited for; matrix products, arithmetic and copies ran while one was open for 2% of the time, Pallas kernels for 0%

commit v1 on v0

v1 whole, which is shorter than its diff:
```python
import functools

import jax
import jax.numpy as jnp
from jax import lax
from jax.experimental import pallas as pl
from jax.experimental.pallas import tpu as pltpu
from jax.sharding import Mesh
from jax.sharding import PartitionSpec as P

MESH = pl.DeviceIdType.MESH
F32 = jnp.float32
BF16 = jnp.bfloat16
TP = ("y", "x")
EPS = 1e-05
ALPHA = 8.0**0.25
NZ, NC, NY, NX = 16, 2, 4, 4
NTP = NY * NX
EXPERTS = NZ * NC
CAP = 48
TOK = 384
MIX_W = 512
FEAT = 2048
FD = 128
HD = 64
LANE = 128
CHUNKS = TOK // LANE
BACK = 4
NG = NZ // NY
PIECES = NG * NC * NY
ORDER = (2, 1, 3, 0)


def dot(a, b, dims=((1,), (0,))):
    return lax.dot_general(a, b, (dims, ((), ())), preferred_element_type=F32)


def iota(shape, dim):
    return lax.broadcasted_iota(jnp.int32, shape, dim)


def turned(row):
    return jnp.broadcast_to(row, (LANE, LANE)).T


def part(value, k):
    return value[:, k * LANE : (k + 1) * LANE]


def rows_of(value, k):
    return value[k * LANE : (k + 1) * LANE]


def remote(src, dst, send, recv, where):
    return pltpu.make_async_remote_copy(
        src_ref=src, dst_ref=dst, send_sem=send, recv_sem=recv, device_id=where, device_id_type=MESH
    )


def norm_columns(totals):
    mean = totals[0:1] / FEAT
    var = totals[1:2] / FEAT - mean * mean
    return mean, lax.rsqrt(var + EPS)


def layer_kernel(
    pool_ref,
    ids_ref,
    pmap_ref,
    scale_ref,
    wout_ref,
    gate_ref,
    res_ref,
    gain1_ref,
    bias1_ref,
    routes_ref,
    rweight_ref,
    wg_hbm,
    wu_hbm,
    wd_hbm,
    gain2_ref,
    bias2_ref,
    out_ref,
    wg_v,
    wu_v,
    halo,
    pk,
    pk_in,
    pg,
    st1,
    st2,
    slots,
    send_rows,
    xb,
    wb,
    db,
    acc,
    hb,
    ob,
    rb,
    pick,
    nat,
    load_sem,
    halo_s,
    halo_r,
    pk_s,
    pk_r,
    pg_s,
    pg_r,
    st1_s,
    st1_r,
    st2_s,
    st2_r,
    disp_s,
    disp_r,
    xf_s,
    xf_r,
    w_s,
    w_r,
    h_s,
    h_r,
    ret_s,
    ret_r,
):
    z, c, y, x = (lax.axis_index(name) for name in ("z", "core", "y", "x"))
    here = (z, c, y, x)
    sp = z * NC + c
    tp = y * NX + x
    right, left = lax.rem(x + 1, NX), lax.rem(x + NX - 1, NX)
    across = lax.rem(x + 2, NX)
    down, up = lax.rem(y + 1, NY), lax.rem(y + NY - 1, NY)
    beyond = lax.rem(y + 2, NY)
    own_piece = (z // NY) * NC * NY + c * NY + y
    shift = lax.rem(y - z + NZ, NY)
    own_self = lax.rem(2 * z, NY) == y

    def sp_device(k):
        return (k // NC, lax.rem(k, NC), y, x)

    def plane_device(k):
        return (z, c, k // NX, lax.rem(k, NX))

    def expert_device(e):
        ze = e // NC
        return (ze, lax.rem(e, NC), lax.rem(z + ze, NY), x)

    def source_device(p):
        g = p // (NC * NY)
        return (g * NY + shift, lax.rem(p // NY, NC), lax.rem(p, NY), x)

    barrier = pltpu.get_barrier_semaphore()

    def greet(device):
        pl.semaphore_signal(barrier, inc=1, device_id=device, device_id_type=MESH)

    @pl.loop(0, NTP)
    def _(k):
        @pl.when(k != tp)
        def _():
            greet(plane_device(k))

    @pl.loop(0, EXPERTS)
    def _(e):
        @pl.when(jnp.logical_not(jnp.logical_and(own_self, e == sp)))
        def _():
            greet(expert_device(e))

    @pl.loop(0, PIECES)
    def _(p):
        @pl.when(jnp.logical_not(jnp.logical_and(own_self, p == own_piece)))
        def _():
            greet(source_device(p))

    for b in range(1, BACK + 1):

        @pl.when(sp + b < EXPERTS)
        def _():
            greet(sp_device(sp + b))

        @pl.when(sp >= b)
        def _():
            greet(sp_device(sp - b))

    loads = [
        pltpu.make_async_copy(wg_hbm, wg_v, load_sem.at[0]),
        pltpu.make_async_copy(wu_hbm, wu_v, load_sem.at[1]),
        pltpu.make_async_copy(wd_hbm, db.at[y], load_sem.at[2]),
    ]
    for load in loads:
        load.start()

    ids = ids_ref[...].astype(F32)
    pool = pool_ref[...]
    last_id = ids[:, TOK - 1 : TOK]
    tail = jnp.broadcast_to((ids == last_id).astype(F32), (8, TOK)).astype(BF16)
    row = iota((LANE, TOK), 0)
    padded = jnp.concatenate([pool, jnp.zeros((LANE - 32, TOK), BF16)], axis=0)
    padded = jnp.where(row == 32, jnp.ones_like(padded), padded)
    sums = dot(tail, padded, ((1,), (1,)))
    line = iota((8, LANE), 0)
    packet = jnp.where(line == 0, sums, jnp.broadcast_to(last_id, (8, LANE)))
    packet = jnp.where(line == 2, jnp.broadcast_to(part(ids, CHUNKS - 1), (8, LANE)), packet)
    pk[...] = packet

    is_doc = x >= 2
    window = jnp.where(is_doc, 4 * TOK, jnp.left_shift(2, y))
    id_col = jnp.concatenate([turned(part(ids, k)) for k in range(CHUNKS)], axis=0)
    sum_own, count_own = [], []
    ones8 = jnp.ones((8, TOK), BF16)
    for k in range(CHUNKS):
        spos = iota((TOK, LANE), 0)
        tpos = iota((TOK, LANE), 1) + k * LANE
        gap = tpos - spos
        keep = (id_col == part(ids, k)) & (gap >= 0) & (gap < window)
        mask = keep.astype(F32).astype(BF16)
        sum_own.append(dot(pool, mask))
        count_own.append(dot(ones8, mask)[0:1])

    expert = iota((EXPERTS, TOK), 0).astype(F32)
    ways = []
    for k in range(2):
        column = jnp.broadcast_to(routes_ref[:, k : k + 1].astype(F32), (TOK, LANE))
        named = jnp.concatenate([rows_of(column, j).T[0:1] for j in range(CHUNKS)], axis=1)
        ways.append((expert == named).astype(F32))
    earlier = (iota((TOK, TOK), 0) < iota((TOK, TOK), 1)).astype(F32).astype(BF16)
    rank = dot((ways[0] + ways[1]).astype(BF16), earlier) + expert * CAP
    for k in range(2):
        slots[k : k + 1, :] = jnp.sum(ways[k] * rank, axis=0, keepdims=True)

    peers = NTP - 1
    partners = 2 * (EXPERTS - own_self.astype(jnp.int32))
    ahead = jnp.minimum(EXPERTS - 1 - sp, BACK)
    behind = jnp.minimum(sp, BACK)
    pl.semaphore_wait(barrier, peers + partners + ahead + behind)

    for b in range(1, BACK + 1):

        @pl.when(sp + b < EXPERTS)
        def _():
            remote(
                pk, pk_in.at[b - 1], pk_s.at[b - 1], pk_r.at[b - 1], sp_device(sp + b)
            ).start()

    edge = pool_ref.at[:, pl.ds(TOK - LANE, LANE)]

    @pl.when(sp + 1 < EXPERTS)
    def _():
        remote(edge, halo, halo_s, halo_r, sp_device(sp + 1)).start()

    wout_t = jnp.concatenate(
        [rows_of(wout_ref[...], k).astype(F32).T for k in range(MIX_W // LANE)], axis=1
    ).astype(BF16)
    gate_t = jnp.concatenate(
        [rows_of(gate_ref[...], k).astype(F32).T for k in range(CHUNKS)], axis=1
    )
    gate_t = jax.nn.sigmoid(gate_t)
    res_t = ALPHA * jnp.concatenate(
        [rows_of(res_ref[...], k).astype(F32).T for k in range(CHUNKS)], axis=1
    )
    none = jnp.zeros((HD, HD), F32)
    maps = []
    for k in range(MIX_W // LANE):
        upper = jnp.concatenate([pmap_ref[2 * k].astype(F32), none], axis=1)
        lower = jnp.concatenate([none, pmap_ref[2 * k + 1].astype(F32)], axis=1)
        maps.append(jnp.concatenate([upper, lower], axis=0).T.astype(BF16))
    scales = [turned(part(scale_ref[...], k)) for k in range(MIX_W // LANE)]
    gain1 = turned(gain1_ref[...])
    bias1 = turned(bias1_ref[...])

    @pl.when(sp >= 1)
    def _():
        remote(edge, halo, halo_s, halo_r, here).wait_recv()

    for b in range(1, BACK + 1):

        @pl.when(sp >= b)
        def _():
            remote(pk, pk_in.at[b - 1], pk_s.at[b - 1], pk_r.at[b - 1], here).wait_recv()

    first_id = jnp.broadcast_to(ids[:, 0:1], (1, LANE))
    carry = jnp.zeros((1, LANE), F32)
    for b in range(1, BACK + 1):
        found = pk_in[b - 1]
        same = (found[1:2] == first_id) & (jnp.broadcast_to(sp, (1, LANE)) >= b)
        carry = carry + jnp.where(same, found[0:1], 0.0)
    carry_col = turned(carry)
    doc_flag = is_doc.astype(F32)
    halo_on = jnp.broadcast_to(jnp.logical_and(sp >= 1, x < 2), (LANE, LANE))
    halo_ids = turned(pk_in[0][2:3])
    gap = iota((LANE, LANE), 1) + LANE - iota((LANE, LANE), 0)
    keep = (halo_ids == part(ids, 0)) & (gap < window) & halo_on
    mask = keep.astype(F32).astype(BF16)
    halo_in = jnp.where(halo_on[0:32], halo[...].astype(F32), 0.0).astype(BF16)
    halo_sum = dot(halo_in, mask)
    halo_count = dot(ones8[:, :LANE], mask)[0:1]
    for k in range(CHUNKS):
        head = (part(ids, k) == first_id).astype(F32) * doc_flag
        total = sum_own[k] + carry_col[0:32] * head
        count = count_own[k] + carry_col[32:33] * head
        if k == 0:
            total = total + halo_sum
            count = count + halo_count
        pooled = total / count - part(pool, k).astype(F32)
        pg[tp, :, k * LANE : (k + 1) * LANE] = pooled.astype(BF16)

    @pl.loop(1, NTP)
    def _(k):
        other = lax.rem(tp + k, NTP)
        remote(pg.at[tp], pg.at[tp], pg_s.at[other], pg_r.at[tp], plane_device(other)).start()

    loads[0].wait()
    loads[1].wait()
    loads[2].wait()
    wb[y] = jnp.concatenate([wg_v[...], wu_v[...]], axis=1)

    @pl.loop(1, NTP)
    def _(k):
        other = lax.rem(tp + k, NTP)
        remote(pg.at[tp], pg.at[other], pg_s.at[other], pg_r.at[other], here).wait_recv()

    mapped = []
    for k in range(MIX_W // LANE):
        grouped = dot(maps[k], pg[4 * k : 4 * k + 4].reshape(LANE, TOK))
        scaled = [part(grouped, j) * scales[k] for j in range(CHUNKS)]
        mapped.append(jnp.concatenate(scaled, axis=1).astype(BF16))
    mixed = res_t + dot(wout_t, jnp.concatenate(mapped, axis=0)) * gate_t
    st1[tp, 0:1] = jnp.sum(mixed, axis=0, keepdims=True)
    st1[tp, 1:2] = jnp.sum(mixed * mixed, axis=0, keepdims=True)

    @pl.loop(1, NTP)
    def _(k):
        other = lax.rem(tp + k, NTP)
        remote(st1.at[tp], st1.at[tp], st1_s.at[other], st1_r.at[tp], plane_device(other)).start()

    @pl.loop(1, NTP)
    def _(k):
        other = lax.rem(tp + k, NTP)
        remote(st1.at[tp], st1.at[other], st1_s.at[other], st1_r.at[other], here).wait_recv()

    mean, rstd = norm_columns(jnp.sum(st1[...], axis=0))
    centred = (mixed - mean) * rstd
    normed = jnp.concatenate(
        [part(centred, k) * gain1 + bias1 for k in range(CHUNKS)], axis=1
    ).astype(BF16)

    for k in range(8):
        first = k * (EXPERTS * CAP // 8)
        place = (iota((EXPERTS * CAP // 8, TOK), 0) + first).astype(F32)
        chosen = (place == slots[0:1, :]) | (place == slots[1:2, :])
        rows = dot(chosen.astype(F32).astype(BF16), normed, ((1,), (1,)))
        send_rows[4 * k : 4 * k + 4] = rows.astype(BF16).reshape(4, CAP, FD)

    for q in ORDER:

        @pl.loop(0, NY * NC)
        def _(k):
            ze = lax.rem(z - k // NC - NY * q + 2 * NZ, NZ)
            e = ze * NC + lax.rem(k, NC)

            @pl.when(jnp.logical_not(jnp.logical_and(own_self, e == sp)))
            def _():
                remote(
                    send_rows.at[e],
                    xb.at[x, z // NY, c, y],
                    disp_s.at[e],
                    disp_r.at[own_piece],
                    expert_device(e),
                ).start()

    @pl.when(own_self)
    def _():
        xb[x, z // NY, c, y] = send_rows[sp]

    def neighbour(yy):
        return (z, c, yy, x)

    def beside(xx):
        return (z, c, y, xx)

    w_own = [
        remote(wb.at[y], wb.at[y], w_s.at[0], w_r.at[0], neighbour(down)),
        remote(wb.at[y], wb.at[y], w_s.at[1], w_r.at[1], neighbour(up)),
        remote(db.at[y], db.at[y], w_s.at[2], w_r.at[2], neighbour(down)),
        remote(db.at[y], db.at[y], w_s.at[3], w_r.at[3], neighbour(up)),
    ]
    for copy in w_own:
        copy.start()

    for k in range(CHUNKS):
        nat[k * LANE : (k + 1) * LANE] = part(normed, k).astype(F32).T
        for way in range(2):
            column = turned(slots[way : way + 1, k * LANE : (k + 1) * LANE])
            for j in range(EXPERTS * CAP // LANE):
                lane = (iota((LANE, LANE), 1) + j * LANE).astype(F32)
                pick[way * TOK + k * LANE : way * TOK + (k + 1) * LANE, j * LANE : (j + 1) * LANE] = (
                    (lane == column).astype(F32).astype(BF16)
                )

    def group_of(q):
        near = lax.rem(y - 2 * z + 2 * NZ, NY)
        return lax.rem(z + near + NY * q, NZ) // NY

    xf = []
    for i, q in enumerate(ORDER):
        g = group_of(q)

        @pl.loop(0, NC * NY)
        def _(k):
            p = g * NC * NY + k

            @pl.when(jnp.logical_not(jnp.logical_and(own_self, p == own_piece)))
            def _():
                remote(
                    send_rows.at[0],
                    xb.at[x, g, k // NY, lax.rem(k, NY)],
                    disp_s.at[0],
                    disp_r.at[p],
                    here,
                ).wait_recv()

        mine = xb.at[x, g]
        to_right = remote(mine, mine, xf_s.at[0, i], xf_r.at[0, i], beside(right))
        to_left = remote(mine, mine, xf_s.at[1, i], xf_r.at[1, i], beside(left))
        to_right.start()
        to_left.start()
        xf += [to_right, to_left]
        if i == 2:
            w_own[0].wait_recv()
            w_own[1].wait_recv()
            half = FEAT // 2
            from_up = wb.at[up, pl.ds(0, half)]
            from_down = wb.at[down, pl.ds(half, half)]
            relays = [
                remote(from_up, from_up, w_s.at[4], w_r.at[4], neighbour(down)),
                remote(from_down, from_down, w_s.at[5], w_r.at[5], neighbour(up)),
            ]
            for copy in relays:
                copy.start()

    for i, q in enumerate(ORDER):
        g = group_of(q)
        xf[2 * i].wait_recv()
        xf[2 * i + 1].wait_recv()
        if i % 2 == 0:
            piece = xb.at[left, g]
            relay = remote(piece, piece, xf_s.at[2, i], xf_r.at[2, i], beside(right))
        else:
            piece = xb.at[right, g]
            relay = remote(piece, piece, xf_s.at[2, i], xf_r.at[2, i], beside(left))
        relay.start()
        xf.append(relay)

    w_own[2].wait_recv()
    w_own[3].wait_recv()
    half = EXPERTS * 16
    from_up = db.at[up, pl.ds(0, half)]
    from_down = db.at[down, pl.ds(half, half)]
    relays += [
        remote(from_up, from_up, w_s.at[6], w_r.at[6], neighbour(down)),
        remote(from_down, from_down, w_s.at[7], w_r.at[7], neighbour(up)),
    ]
    relays[2].start()
    relays[3].start()

    relays[0].wait_recv()
    relays[1].wait_recv()

    def projected(xx):
        tiles, weights = [], []
        for yy in range(NY):
            tiles.append(xb[xx, :, :, yy].reshape(TOK, FD))
            start = pl.multiple_of((yy * NX + xx) * FD, FD)
            weights.append(
                jnp.concatenate([wb[b, pl.ds(start, FD), :] for b in range(NY)], axis=1)
            )
        return dot(jnp.concatenate(tiles, axis=1), jnp.concatenate(weights, axis=0))

    acc[...] = projected(x)
    acc[...] += projected(left)
    acc[...] += projected(right)
    for i in range(NG):
        xf[2 * NG + i].wait_recv()
    acc[...] += projected(across)

    low = iota((TOK, LANE), 1) < HD
    for pair in range(NY // 2):
        one = acc[:, 2 * pair * LANE : (2 * pair + 1) * LANE]
        two = acc[:, (2 * pair + 1) * LANE : (2 * pair + 2) * LANE]
        gate = jnp.where(low, one, pltpu.roll(two, HD, 1))
        lift = jnp.where(low, pltpu.roll(one, HD, 1), two)
        hidden = gate * jax.nn.sigmoid(gate) * lift
        hb[x, :, pair * LANE : (pair + 1) * LANE] = hidden.astype(BF16)

    mine = hb.at[x]
    h_right = remote(mine, mine, h_s.at[0], h_r.at[0], beside(right))
    h_left = remote(mine, mine, h_s.at[1], h_r.at[1], beside(left))
    h_right.start()
    h_left.start()
    relays[2].wait_recv()
    relays[3].wait_recv()

    def lowered(xx):
        blocks = []
        for yy in range(NY):
            pieces = [
                db[yy, pl.ds(pl.multiple_of((b * NX + xx) * HD, HD), HD), :] for b in range(NY)
            ]
            blocks.append(jnp.concatenate(pieces, axis=0))
        return dot(hb[xx], jnp.concatenate(blocks, axis=1))

    acc[...] = lowered(x)
    half = TOK // 2
    h_right.wait_recv()
    piece = hb.at[left, pl.ds(0, half)]
    h_first = remote(piece, piece, h_s.at[2], h_r.at[2], beside(right))
    h_first.start()
    h_left.wait_recv()
    piece = hb.at[right, pl.ds(half, half)]
    h_second = remote(piece, piece, h_s.at[3], h_r.at[3], beside(left))
    h_second.start()
    acc[...] += lowered(left)
    acc[...] += lowered(right)
    h_first.wait_recv()
    h_second.wait_recv()
    result = (acc[...] + lowered(across)).astype(BF16)
    for yy in range(NY):
        ob[:, :, yy] = part(result, yy).reshape(NG, NC, CAP, FD)

    for q in ORDER:
        g = group_of(q)

        @pl.loop(0, NC * NY)
        def _(k):
            p = g * NC * NY + k

            @pl.when(jnp.logical_not(jnp.logical_and(own_self, p == own_piece)))
            def _():
                remote(
                    ob.at[g, k // NY, lax.rem(k, NY)],
                    rb.at[sp],
                    ret_s.at[p],
                    ret_r.at[sp],
                    source_device(p),
                ).start()

    @pl.when(own_self)
    def _():
        rb[sp] = ob[z // NY, c, y]

    @pl.loop(0, EXPERTS)
    def _(e):
        @pl.when(jnp.logical_not(jnp.logical_and(own_self, e == sp)))
        def _():
            remote(ob.at[0, 0, 0], rb.at[e], ret_s.at[0], ret_r.at[e], here).wait_recv()

    picked = dot(pick[...], rb[...].reshape(EXPERTS * CAP, FD))
    final = (
        ALPHA * nat[...]
        + picked[:TOK] * rweight_ref[:, 0:1]
        + picked[TOK:] * rweight_ref[:, 1:2]
    )
    for k in range(CHUNKS):
        block = rows_of(final, k).T
        st2[tp, 0:1, k * LANE : (k + 1) * LANE] = jnp.sum(block, axis=0, keepdims=True)
        st2[tp, 1:2, k * LANE : (k + 1) * LANE] = jnp.sum(block * block, axis=0, keepdims=True)

    @pl.loop(1, NTP)
    def _(k):
        other = lax.rem(tp + k, NTP)
        remote(st2.at[tp], st2.at[tp], st2_s.at[other], st2_r.at[tp], plane_device(other)).start()

    @pl.loop(1, NTP)
    def _(k):
        other = lax.rem(tp + k, NTP)
        remote(st2.at[tp], st2.at[other], st2_s.at[other], st2_r.at[other], here).wait_recv()

    mean, rstd = norm_columns(jnp.sum(st2[...], axis=0))
    for k in range(CHUNKS):
        centred = (rows_of(final, k) - turned(part(mean, k))) * turned(part(rstd, k))
        out_ref[k * LANE : (k + 1) * LANE, :] = (
            centred * gain2_ref[...] + bias2_ref[...]
        ).astype(BF16)

    for b in range(1, BACK + 1):

        @pl.when(sp + b < EXPERTS)
        def _():
            remote(pk, pk_in.at[b - 1], pk_s.at[b - 1], pk_r.at[b - 1], here).wait_send()

    @pl.when(sp + 1 < EXPERTS)
    def _():
        remote(edge, halo, halo_s, halo_r, here).wait_send()

    @pl.loop(1, NTP)
    def _(k):
        other = lax.rem(tp + k, NTP)
        remote(pg.at[tp], pg.at[tp], pg_s.at[other], pg_r.at[tp], here).wait_send()
        remote(st1.at[tp], st1.at[tp], st1_s.at[other], st1_r.at[tp], here).wait_send()
        remote(st2.at[tp], st2.at[tp], st2_s.at[other], st2_r.at[tp], here).wait_send()

    @pl.loop(0, EXPERTS)
    def _(e):
        @pl.when(jnp.logical_not(jnp.logical_and(own_self, e == sp)))
        def _():
            remote(send_rows.at[e], rb.at[0], disp_s.at[e], disp_r.at[0], here).wait_send()

        @pl.when(jnp.logical_not(jnp.logical_and(own_self, e == own_piece)))
        def _():
            remote(ob.at[0, 0, 0], rb.at[0], ret_s.at[e], ret_r.at[0], here).wait_send()

    for copy in xf + w_own + relays + [h_right, h_left, h_first, h_second]:
        copy.wait_send()


def body(
    pool_in,
    doc_ids,
    pool_map,
    pool_scale,
    w_out,
    gate_logit,
    residual,
    first_gain,
    first_bias,
    routes,
    route_weight,
    w_gate,
    w_up,
    w_down,
    second_gain,
    second_bias,
):
    vmem = pl.BlockSpec(memory_space=pltpu.VMEM)
    hbm = pl.BlockSpec(memory_space=pl.ANY)
    dma = pltpu.SemaphoreType.DMA
    args = (
        pool_in,
        doc_ids.reshape(1, -1),
        pool_map,
        pool_scale.reshape(1, -1),
        w_out,
        gate_logit,
        residual,
        first_gain.reshape(1, -1),
        first_bias.reshape(1, -1),
        routes,
        route_weight,
        w_gate[0],
        w_up[0],
        w_down[0],
        second_gain.reshape(1, -1),
        second_bias.reshape(1, -1),
    )
    in_specs = [vmem] * 11 + [hbm] * 3 + [vmem] * 2
    return pl.pallas_call(
        layer_kernel,
        out_shape=jax.ShapeDtypeStruct((TOK, FD), BF16),
        in_specs=in_specs,
        out_specs=vmem,
        scratch_shapes=[
            pltpu.VMEM((FEAT, HD), BF16),
            pltpu.VMEM((FEAT, HD), BF16),
            pltpu.VMEM((32, LANE), BF16),
            pltpu.VMEM((8, LANE), F32),
            pltpu.VMEM((BACK, 8, LANE), F32),
            pltpu.VMEM((NTP, 32, TOK), BF16),
            pltpu.VMEM((NTP, 2, TOK), F32),
            pltpu.VMEM((NTP, 2, TOK), F32),
            pltpu.VMEM((8, TOK), F32),
            pltpu.VMEM((EXPERTS, CAP, FD), BF16),
            pltpu.VMEM((NX, NG, NC, NY, CAP, FD), BF16),
            pltpu.VMEM((NY, FEAT, 2 * HD), BF16),
            pltpu.VMEM((NY, NTP * HD, FD), BF16),
            pltpu.VMEM((TOK, NY * LANE), F32),
            pltpu.VMEM((NX, TOK, NY * HD), BF16),
            pltpu.VMEM((NG, NC, NY, CAP, FD), BF16),
            pltpu.VMEM((EXPERTS, CAP, FD), BF16),
            pltpu.VMEM((2 * TOK, EXPERTS * CAP), BF16),
            pltpu.VMEM((TOK, FD), F32),
            dma((3,)),
            dma,
            dma,
            dma((BACK,)),
            dma((BACK,)),
            dma((NTP,)),
            dma((NTP,)),
            dma((NTP,)),
            dma((NTP,)),
            dma((NTP,)),
            dma((NTP,)),
            dma((EXPERTS,)),
            dma((PIECES,)),
            dma((3, NG)),
            dma((3, NG)),
            dma((8,)),
            dma((8,)),
            dma((4,)),
            dma((4,)),
            dma((PIECES,)),
            dma((EXPERTS,)),
        ],
        compiler_params=pltpu.CompilerParams(
            collective_id=0, has_side_effects=True, vmem_limit_bytes=48 * 1024 * 1024
        ),
        cost_estimate=pl.CostEstimate(
            flops=2_000_000_000, bytes_accessed=4_000_000, transcendentals=0
        ),
        name="layer",
    )(*args)


def solution(mesh):
    finer = Mesh(mesh.devices.reshape(NZ, NC, NY, NX), ("z", "core", "y", "x"))
    sp = ("z", "core")
    in_specs = (
        P(TP, sp),
        P(sp),
        P(),
        P(),
        P(None, TP),
        P(sp, TP),
        P(sp, TP),
        P(TP),
        P(TP),
        P(sp, None),
        P(sp, None),
        P(sp, None, TP),
        P(sp, None, TP),
        P(sp, None, TP),
        P(TP),
        P(TP),
    )
    return jax.shard_map(
        body, mesh=finer, in_specs=in_specs, out_specs=P(sp, TP), check_vma=False
    )
```

time: 346 us -> 114 us (0.33)
  waiting for transfers between devices: 163 us -> 0 us
  Pallas kernels: 0 us -> 108 us
  blocking collectives: 78.8 us -> 0 us
  starting transfers between devices: 39.4 us -> 0 us
  between operations: 19 us -> 0.14 us
  local copies, waits for them, and re-layouts: 22.3 us -> 5.02 us
  matrix products: 11.3 us -> 0 us
  other arithmetic: 8.31 us -> 0 us
    all_gather x2 -> x0, waiting for transfers between devices: 118 us -> none  [the longest x1 68.3 us: body(): inputs = lax.all_gather(arrived, TP, axis=1, tiled=True)]
    pallas_call x0 -> x1, Pallas kernels: none -> 108 us  [body(): pl.pallas_call(layer_kernel, out_shape=jax.ShapeDtypeStruct((TOK, FD), BF...]
    all_to_all x3 -> x0, waiting for transfers between devices: 44.6 us -> none  [the longest x1 27.6 us: body(): lax.all_to_all(result.astype(jnp.bfloat16), 'sp', split_axis=0, concat_ax...]
    all_to_all x1 -> x0, blocking collectives: 38 us -> none  [body(): lax.all_to_all(outgoing, 'sp', split_axis=0, concat_axis=0, tiled=True)]
    all_to_all x3 -> x0, starting transfers between devices: 34.2 us -> none  [the longest x2 21 us: copy_for_each(): return lax.all_to_all(copies, axis, split_axis=0, concat_axis=0, tiled=True)]
    psum x4 -> x0, blocking collectives: 28.4 us -> none  [over_axes(): return functools.reduce(lax.psum, axes, shard)]
    all_gather x1 -> x0, blocking collectives: 12.4 us -> none  [gathered_by_axis(): out = lax.all_gather(out, axes[number], axis=dim, tiled=True)]
    dot_general x5 -> x0, matrix products: 11.3 us -> none  [the longest x1 4.95 us: body(): gate_part = jnp.dot(inputs, w_gate[0], preferred_element_type=jnp.float32)]
  transfers between devices with their start and end apart: 6 -> 0, of which waited for: 6 -> 0; matrix products, arithmetic and copies ran while one was open for 2% -> 0% of each run, Pallas kernels for 0% -> 0%
where the time goes in v1:
time: 114 us; the launch traced here: 113 us
  Pallas kernels  108 us (95%)
  local copies, waits for them, and re-layouts  5.02 us (4%)
    pallas_call x1, Pallas kernels, body(): pl.pallas_call(layer_kernel, out_shape=jax.ShapeDtypeStruct((TOK, FD), BF...  108 us
    unnamed x31, local copies, waits for them, and re-layouts  4.29 us

profile of v1, /device:TPU:1, one launch (start us, length us, event | category | flops | bytes accessed | tf_op | source)
XLA Modules:
  0.0 113.5 jit_solution(2648303725633636298)
XLA Ops:
  0.0 0.0 copy-start.11
  0.0 0.7 reshape.18.ids_ref
  0.7 0.8 copy.19.routes_ref
  1.6 0.8 copy.20.rweight_ref
  2.4 0.0 copy-done.11
  2.4 0.0 copy-start.12
  2.4 0.3 copy.17
  2.7 0.7 copy-done.12
  3.3 0.0 copy-start
  3.3 0.0 copy-start.1
  3.3 0.0 copy-start.2
  3.4 0.0 copy-start.4
  3.4 0.0 copy-start.5
  3.4 0.0 copy-start.6
  3.4 0.0 copy-start.10
  3.4 0.3 copy.18
  3.7 0.0 copy-start.7
  3.7 0.0 copy-start.8
  3.7 0.0 copy-start.9
  3.7 0.6 copy-done
  4.3 0.0 copy-done.1
  4.3 0.1 copy-done.2
  4.4 0.1 copy-done.3
  4.4 0.0 copy-done.4
  4.5 0.0 copy-done.5
  4.5 0.0 copy-done.6
  4.5 0.0 copy-done.10
  4.5 0.0 copy-done.7
  4.5 0.0 copy-done.8
  4.5 0.0 copy-done.9
  4.5 108.3 %layer.1 = bf16[384,128]{1,0:T(8,128)(2,1)S(1)} custom-call(bf16[32,384]{1,0:T(8,128)(2,1)S(1)} %copy-done.5, s32[1,384]{1,0:T(1,128)S(1)} %reshape.18.ids_ref, bf16[8,64,64]{2,1,0:T(8,128)(2,1)S(1)} %copy-done.1, f32[1,512]{1,0:T(1,128)S(1)} %bitcast.11, bf16[512,128]{1,0:T(8,128)(2,1)S(1)} %copy-done.2, bf16[384,128]{1,0:T(8,128)(2,1)S(1)} %copy-done.3, ...), custom_call_target="tpu_custom_call" | custom-call | flops 2000000000 | bytes 4000000 | tf_op jit(solution)/shard_map/layer/pallas_call | solution.py:655
  112.8 0.6 copy.22
  (1 shorter events, 0.0 us)
Async XLA Ops:
  0.0 2.4 %copy-start.11 = (bf16[1,2048,64]{1,2,0:T(8,128)(2,1)S(1)}, bf16[1,2048,64]{1,2,0:T(8,128)(2,1)}, u32[]{:S(2)}) copy-start(bf16[1,2048,64]{1,2,0:T(8,128)(2,1)} %param.27) | copy-start | bytes 786436
  2.4 1.0 copy-start.12
  3.3 0.9 copy-start
  3.3 1.0 copy-start.1
  3.3 1.0 copy-start.2
  3.3 1.1 copy-start.3
  3.4 1.1 copy-start.4
  3.4 1.1 copy-start.5
  3.4 1.1 copy-start.6
  3.4 1.1 copy-start.10
  3.7 0.8 copy-start.7
  3.7 0.8 copy-start.8
  3.7 0.8 copy-start.9

commit v2 on v1

v2 whole, which is shorter than its diff:
```python
import functools

import jax
import jax.numpy as jnp
from jax import lax
from jax.experimental import pallas as pl
from jax.experimental.pallas import tpu as pltpu
from jax.sharding import Mesh
from jax.sharding import PartitionSpec as P

MESH = pl.DeviceIdType.MESH
F32 = jnp.float32
BF16 = jnp.bfloat16
TP = ("y", "x")
EPS = 1e-05
ALPHA = 8.0**0.25
NZ, NC, NY, NX = 16, 2, 4, 4
NTP = NY * NX
EXPERTS = NZ * NC
CAP = 48
TOK = 384
MIX_W = 512
FEAT = 2048
FD = 128
HD = 64
LANE = 128
CHUNKS = TOK // LANE
BACK = 4
NG = NZ // NY
PIECES = NG * NC * NY
ORDER = (2, 1, 3, 0)


def dot(a, b, dims=((1,), (0,))):
    return lax.dot_general(a, b, (dims, ((), ())), preferred_element_type=F32)


def iota(shape, dim):
    return lax.broadcasted_iota(jnp.int32, shape, dim)


def turned(row):
    return jnp.broadcast_to(row, (LANE, LANE)).T


def part(value, k):
    return value[:, k * LANE : (k + 1) * LANE]


def rows_of(value, k):
    return value[k * LANE : (k + 1) * LANE]


def remote(src, dst, send, recv, where):
    return pltpu.make_async_remote_copy(
        src_ref=src, dst_ref=dst, send_sem=send, recv_sem=recv, device_id=where, device_id_type=MESH
    )


def norm_columns(totals):
    mean = totals[0:1] / FEAT
    var = totals[1:2] / FEAT - mean * mean
    return mean, lax.rsqrt(var + EPS)


def layer_kernel(
    pool_h,
    ids_h,
    pmap_h,
    scale_h,
    wout_h,
    gate_h,
    res_h,
    gain1_h,
    bias1_h,
    routes_h,
    rweight_h,
    wg_h,
    wu_h,
    wd_h,
    gain2_h,
    bias2_h,
    out_ref,
    pool_ref,
    ids_ref,
    pmap_ref,
    scale_ref,
    wout_ref,
    gate_ref,
    res_ref,
    gain1_ref,
    bias1_ref,
    routes_ref,
    rweight_ref,
    gain2_ref,
    bias2_ref,
    halo,
    pk,
    pk_in,
    pg,
    st1,
    st2,
    slots,
    send_rows,
    xb,
    wb,
    db,
    acc,
    hb,
    ob,
    rb,
    pick,
    nat,
    load_sem,
    near_sem,
    far_sem,
    halo_s,
    halo_r,
    pk_s,
    pk_r,
    pg_s,
    pg_r,
    st1_s,
    st1_r,
    st2_s,
    st2_r,
    disp_s,
    disp_r,
    xf_s,
    xf_r,
    w_s,
    w_r,
    h_s,
    h_r,
    ret_s,
    ret_r,
):
    z, c, y, x = (lax.axis_index(name) for name in ("z", "core", "y", "x"))
    here = (z, c, y, x)
    sp = z * NC + c
    tp = y * NX + x
    right, left = lax.rem(x + 1, NX), lax.rem(x + NX - 1, NX)
    across = lax.rem(x + 2, NX)
    down, up = lax.rem(y + 1, NY), lax.rem(y + NY - 1, NY)
    near = lax.rem(y - 2 * z + 2 * NZ, NY)
    own_self = near == 0
    own_place = c * NY + y

    def sp_device(k):
        return (k // NC, lax.rem(k, NC), y, x)

    def plane_device(k):
        return (z, c, k // NX, lax.rem(k, NX))

    def line_device(dz):
        return (lax.rem(z + dz + NZ, NZ), c, y, x)

    def expert_device(e):
        ze = e // NC
        return (ze, lax.rem(e, NC), lax.rem(z + ze, NY), x)

    def source_device(q, k):
        return (lax.rem(z + near + NY * q, NZ), k // NY, lax.rem(k, NY), x)

    def neighbour(yy):
        return (z, c, yy, x)

    def beside(xx):
        return (z, c, y, xx)

    def signal(sem, device):
        pl.semaphore_signal(sem, inc=1, device_id=device, device_id_type=MESH)

    loads = [
        pltpu.make_async_copy(src, dst, load_sem.at[k])
        for k, (src, dst) in enumerate(
            [
                (pool_h, pool_ref),
                (ids_h, ids_ref),
                (routes_h, routes_ref),
                (wg_h, wb.at[y, pl.ds(0, HD)]),
                (wu_h, wb.at[y, pl.ds(HD, HD)]),
                (wout_h, wout_ref),
                (gate_h, gate_ref),
                (res_h, res_ref),
                (pmap_h, pmap_ref),
                (scale_h, scale_ref),
                (gain1_h, gain1_ref),
                (bias1_h, bias1_ref),
                (wd_h, db.at[y]),
                (rweight_h, rweight_ref),
                (gain2_h, gain2_ref),
                (bias2_h, bias2_ref),
            ]
        )
    ]
    for load in loads:
        load.start()
    barrier = pltpu.get_barrier_semaphore()
    for dz in range(-2, 3):
        for other in range(NC):
            if dz:
                signal(barrier, (lax.rem(z + dz + NZ, NZ), other, y, x))
    signal(barrier, (z, 1 - c, y, x))

    @pl.loop(1, NTP)
    def _(k):
        signal(barrier, plane_device(lax.rem(tp + k, NTP)))

    loads[0].wait()
    loads[1].wait()
    ids = [ids_ref[k : k + 1, :].astype(F32) for k in range(CHUNKS)]
    pool = pool_ref[...]
    last_id = ids[CHUNKS - 1][:, LANE - 1 : LANE]
    tail = jnp.concatenate([(line == last_id).astype(F32) for line in ids], axis=1)
    tail = jnp.broadcast_to(tail, (8, TOK)).astype(BF16)
    padded = jnp.concatenate([pool, jnp.zeros((LANE - 32, TOK), BF16)], axis=0)
    padded = jnp.where(iota((LANE, TOK), 0) == 32, jnp.ones_like(padded), padded)
    sums = dot(tail, padded, ((1,), (1,)))
    line = iota((8, LANE), 0)
    packet = jnp.where(line == 0, sums, jnp.broadcast_to(last_id, (8, LANE)))
    packet = jnp.where(line == 2, jnp.broadcast_to(ids[CHUNKS - 1], (8, LANE)), packet)
    pk[...] = packet

    is_doc = x >= 2
    window = jnp.where(is_doc, 4 * TOK, jnp.left_shift(2, y))
    id_col = jnp.concatenate([turned(ids[k]) for k in range(CHUNKS)], axis=0)
    sum_own, count_own = [], []
    ones8 = jnp.ones((8, TOK), BF16)
    for k in range(CHUNKS):
        gap = iota((TOK, LANE), 1) + k * LANE - iota((TOK, LANE), 0)
        keep = (id_col == ids[k]) & (gap >= 0) & (gap < window)
        mask = keep.astype(F32).astype(BF16)
        sum_own.append(dot(pool, mask))
        count_own.append(dot(ones8, mask)[0:1])

    pl.semaphore_wait(barrier, NTP - 1 + 5 * NC - 1)

    for b in range(1, BACK + 1):

        @pl.when(sp + b < EXPERTS)
        def _():
            remote(
                pk, pk_in.at[b - 1], pk_s.at[b - 1], pk_r.at[b - 1], sp_device(sp + b)
            ).start()

    edge = pool_ref.at[:, pl.ds(TOK - LANE, LANE)]

    @pl.when(sp + 1 < EXPERTS)
    def _():
        remote(edge, halo, halo_s, halo_r, sp_device(sp + 1)).start()

    signal(near_sem, line_device(2))
    signal(near_sem, line_device(-2))

    weights = []

    def send_weights(source, first, count):
        k = 2 * len(weights)
        block = source.at[y, pl.ds(first, count)]
        pair = [
            remote(block, block, w_s.at[k], w_r.at[k], neighbour(down)),
            remote(block, block, w_s.at[k + 1], w_r.at[k + 1], neighbour(up)),
        ]
        for copy in pair:
            copy.start()
        weights.append(pair)

    loads[3].wait()
    loads[4].wait()
    send_weights(wb, 0, 32)

    for k in (2, *range(5, len(loads))):
        loads[k].wait()
    wout_t = jnp.concatenate(
        [rows_of(wout_ref[...], k).astype(F32).T for k in range(MIX_W // LANE)], axis=1
    ).astype(BF16)
    gate_t = jnp.concatenate(
        [rows_of(gate_ref[...], k).astype(F32).T for k in range(CHUNKS)], axis=1
    )
    gate_t = jax.nn.sigmoid(gate_t)
    res_t = ALPHA * jnp.concatenate(
        [rows_of(res_ref[...], k).astype(F32).T for k in range(CHUNKS)], axis=1
    )
    none = jnp.zeros((HD, HD), F32)
    maps = []
    for k in range(MIX_W // LANE):
        upper = jnp.concatenate([pmap_ref[2 * k].astype(F32), none], axis=1)
        lower = jnp.concatenate([none, pmap_ref[2 * k + 1].astype(F32)], axis=1)
        maps.append(jnp.concatenate([upper, lower], axis=0).T.astype(BF16))
    scales = [turned(part(scale_ref[...], k)) for k in range(MIX_W // LANE)]
    gain1 = turned(gain1_ref[...])
    bias1 = turned(bias1_ref[...])

    @pl.when(sp >= 1)
    def _():
        remote(edge, halo, halo_s, halo_r, here).wait_recv()

    for b in range(1, BACK + 1):

        @pl.when(sp >= b)
        def _():
            remote(pk, pk_in.at[b - 1], pk_s.at[b - 1], pk_r.at[b - 1], here).wait_recv()

    first_id = jnp.broadcast_to(ids[0][:, 0:1], (1, LANE))
    carry = jnp.zeros((1, LANE), F32)
    for b in range(1, BACK + 1):
        found = pk_in[b - 1]
        same = (found[1:2] == first_id) & (jnp.broadcast_to(sp, (1, LANE)) >= b)
        carry = carry + jnp.where(same, found[0:1], 0.0)
    carry_col = turned(carry)
    doc_flag = is_doc.astype(F32)
    halo_on = jnp.broadcast_to(jnp.logical_and(sp >= 1, x < 2), (LANE, LANE))
    halo_ids = turned(pk_in[0][2:3])
    gap = iota((LANE, LANE), 1) + LANE - iota((LANE, LANE), 0)
    keep = (halo_ids == ids[0]) & (gap < window) & halo_on
    mask = keep.astype(F32).astype(BF16)
    halo_in = jnp.where(halo_on[0:32], halo[...].astype(F32), 0.0).astype(BF16)
    halo_sum = dot(halo_in, mask)
    halo_count = dot(ones8[:, :LANE], mask)[0:1]
    for k in range(CHUNKS):
        head = (ids[k] == first_id).astype(F32) * doc_flag
        total = sum_own[k] + carry_col[0:32] * head
        count = count_own[k] + carry_col[32:33] * head
        if k == 0:
            total = total + halo_sum
            count = count + halo_count
        pooled = total / count - part(pool, k).astype(F32)
        pg[tp, :, k * LANE : (k + 1) * LANE] = pooled.astype(BF16)

    @pl.loop(1, NTP)
    def _(k):
        other = lax.rem(tp + k, NTP)
        remote(pg.at[tp], pg.at[tp], pg_s.at[other], pg_r.at[tp], plane_device(other)).start()

    send_weights(wb, 32, 16)
    pl.semaphore_wait(near_sem, 2)
    signal(far_sem, line_device(4))
    signal(far_sem, line_device(-4))

    expert = iota((EXPERTS, TOK), 0).astype(F32)
    ways = [(expert == routes_ref[k : k + 1, :].astype(F32)).astype(F32) for k in range(2)]
    earlier = (iota((TOK, TOK), 0) < iota((TOK, TOK), 1)).astype(F32).astype(BF16)
    rank = dot((ways[0] + ways[1]).astype(BF16), earlier) + expert * CAP
    for k in range(2):
        slots[k : k + 1, :] = jnp.sum(ways[k] * rank, axis=0, keepdims=True)

    @pl.loop(1, NTP)
    def _(k):
        other = lax.rem(tp + k, NTP)
        remote(pg.at[tp], pg.at[other], pg_s.at[other], pg_r.at[other], here).wait_recv()

    mapped = []
    for k in range(MIX_W // LANE):
        grouped = dot(maps[k], pg[4 * k : 4 * k + 4].reshape(LANE, TOK))
        scaled = [part(grouped, j) * scales[k] for j in range(CHUNKS)]
        mapped.append(jnp.concatenate(scaled, axis=1).astype(BF16))
    mixed = res_t + dot(wout_t, jnp.concatenate(mapped, axis=0)) * gate_t
    st1[tp, 0:1] = jnp.sum(mixed, axis=0, keepdims=True)
    st1[tp, 1:2] = jnp.sum(mixed * mixed, axis=0, keepdims=True)

    pl.semaphore_wait(far_sem, 2)

    @pl.loop(1, NTP)
    def _(k):
        other = lax.rem(tp + k, NTP)
        remote(st1.at[tp], st1.at[tp], st1_s.at[other], st1_r.at[tp], plane_device(other)).start()

    send_weights(wb, 48, 64)

    @pl.loop(1, NTP)
    def _(k):
        other = lax.rem(tp + k, NTP)
        remote(st1.at[tp], st1.at[other], st1_s.at[other], st1_r.at[other], here).wait_recv()

    mean, rstd = norm_columns(jnp.sum(st1[...], axis=0))
    centred = (mixed - mean) * rstd
    normed = jnp.concatenate(
        [part(centred, k) * gain1 + bias1 for k in range(CHUNKS)], axis=1
    ).astype(BF16)

    for k in range(8):
        first = k * (EXPERTS * CAP // 8)
        place = (iota((EXPERTS * CAP // 8, TOK), 0) + first).astype(F32)
        chosen = (place == slots[0:1, :]) | (place == slots[1:2, :])
        rows = dot(chosen.astype(F32).astype(BF16), normed, ((1,), (1,)))
        send_rows[4 * k : 4 * k + 4] = rows.astype(BF16).reshape(4, CAP, FD)

    for q in ORDER:

        @pl.loop(0, NY * NC)
        def _(k):
            ze = lax.rem(z - k // NC - NY * q + 2 * NZ, NZ)
            e = ze * NC + lax.rem(k, NC)

            @pl.when(jnp.logical_not(jnp.logical_and(own_self, e == sp)))
            def _():
                remote(
                    send_rows.at[e],
                    xb.at[x, q, c, y],
                    disp_s.at[e],
                    disp_r.at[q, own_place],
                    expert_device(e),
                ).start()

    @pl.when(own_self)
    def _():
        xb[x, 0, c, y] = send_rows[sp]

    send_weights(wb, 112, 16)
    send_weights(db, 0, NTP * HD)

    for k in range(CHUNKS):
        nat[k * LANE : (k + 1) * LANE] = part(normed, k).astype(F32).T
        for way in range(2):
            column = turned(slots[way : way + 1, k * LANE : (k + 1) * LANE])
            for j in range(EXPERTS * CAP // LANE):
                lane = (iota((LANE, LANE), 1) + j * LANE).astype(F32)
                pick[way * TOK + k * LANE : way * TOK + (k + 1) * LANE, j * LANE : (j + 1) * LANE] = (
                    (lane == column).astype(F32).astype(BF16)
                )

    relays = []

    def relay_weights(source, count):
        k = 2 * len(weights) + len(relays)
        from_up = source.at[up, pl.ds(0, count)]
        from_down = source.at[down, pl.ds(count, count)]
        pair = [
            remote(from_up, from_up, w_s.at[k], w_r.at[k], neighbour(down)),
            remote(from_down, from_down, w_s.at[k + 1], w_r.at[k + 1], neighbour(up)),
        ]
        for copy in pair:
            copy.start()
        relays.extend(pair)

    def wait_weights(first, last):
        for pair in weights[first:last]:
            for copy in pair:
                copy.wait_recv()

    xf, xr = {}, {}

    def arrive(q):
        @pl.loop(0, NC * NY)
        def _(k):
            mine = jnp.logical_and(own_self, k == own_place) if q == 0 else jnp.bool_(False)

            @pl.when(jnp.logical_not(mine))
            def _():
                remote(
                    send_rows.at[0],
                    xb.at[x, q, k // NY, lax.rem(k, NY)],
                    disp_s.at[0],
                    disp_r.at[q, k],
                    here,
                ).wait_recv()

        mine = xb.at[x, q]
        xf[q] = [
            remote(mine, mine, xf_s.at[0, q], xf_r.at[0, q], beside(right)),
            remote(mine, mine, xf_s.at[1, q], xf_r.at[1, q], beside(left)),
        ]
        for copy in xf[q]:
            copy.start()

    def relay_rows(q, to_right):
        for copy in xf[q]:
            copy.wait_recv()
        piece = xb.at[left if to_right else right, q]
        xr[q] = remote(
            piece, piece, xf_s.at[2, q], xf_r.at[2, q], beside(right if to_right else left)
        )
        xr[q].start()

    def projected(pair, xx):
        tiles, columns = [], []
        for yy in range(NY):
            block = [xb[xx, q, :, yy].reshape(NC * CAP, FD) for q in pair]
            tiles.append(jnp.concatenate(block, axis=0))
            start = pl.multiple_of((yy * NX + xx) * FD, FD)
            columns.append(
                jnp.concatenate([wb[b, :, pl.ds(start, FD)] for b in range(NY)], axis=0)
            )
        return dot(
            jnp.concatenate(tiles, axis=1), jnp.concatenate(columns, axis=1), ((1,), (1,))
        )

    half = TOK // 2
    low = iota((half, LANE), 1) < HD

    def hidden_rows(number, pair):
        for q in pair:
            xr[q].wait_recv()
        acc[...] = projected(pair, x)
        for xx in (left, right, across):
            acc[...] += projected(pair, xx)
        for k in range(NY // 2):
            one = acc[:, 2 * k * LANE : (2 * k + 1) * LANE]
            two = acc[:, (2 * k + 1) * LANE : (2 * k + 2) * LANE]
            gate = jnp.where(low, one, pltpu.roll(two, HD, 1))
            lift = jnp.where(low, pltpu.roll(one, HD, 1), two)
            hidden = gate * jax.nn.sigmoid(gate) * lift
            hb[x, number, :, k * LANE : (k + 1) * LANE] = hidden.astype(BF16)
        mine = hb.at[x, number]
        copies = [
            remote(mine, mine, h_s.at[number, 0], h_r.at[number, 0], beside(right)),
            remote(mine, mine, h_s.at[number, 1], h_r.at[number, 1], beside(left)),
        ]
        for copy in copies:
            copy.start()
        return copies

    def relay_hidden(number, copies):
        copies[0].wait_recv()
        piece = hb.at[left, number, pl.ds(0, half // 2)]
        first = remote(piece, piece, h_s.at[number, 2], h_r.at[number, 2], beside(right))
        first.start()
        copies[1].wait_recv()
        piece = hb.at[right, number, pl.ds(half // 2, half // 2)]
        second = remote(piece, piece, h_s.at[number, 3], h_r.at[number, 3], beside(left))
        second.start()
        copies += [first, second]

    def lowered(number, xx):
        blocks = []
        for yy in range(NY):
            pieces = [
                db[yy, pl.ds(pl.multiple_of((b * NX + xx) * HD, HD), HD), :] for b in range(NY)
            ]
            blocks.append(jnp.concatenate(pieces, axis=0))
        return dot(hb[xx, number], jnp.concatenate(blocks, axis=1))

    def give_back(number, pair, copies):
        acc[...] = lowered(number, x)
        acc[...] += lowered(number, left)
        acc[...] += lowered(number, right)
        copies[2].wait_recv()
        copies[3].wait_recv()
        result = (acc[...] + lowered(number, across)).astype(BF16)
        for k, q in enumerate(pair):
            rows = result[k * NC * CAP : (k + 1) * NC * CAP]
            for yy in range(NY):
                ob[q, :, yy] = part(rows, yy).reshape(NC, CAP, FD)

            @pl.loop(0, NC * NY)
            def _(k):
                mine = jnp.logical_and(own_self, k == own_place) if q == 0 else jnp.bool_(False)

                @pl.when(jnp.logical_not(mine))
                def _():
                    remote(
                        ob.at[q, k // NY, lax.rem(k, NY)],
                        rb.at[sp],
                        ret_s.at[q, k],
                        ret_r.at[sp],
                        source_device(q, k),
                    ).start()

    far_half, near_half = ORDER[:2], ORDER[2:]
    arrive(far_half[0])
    arrive(far_half[1])
    wait_weights(0, 4)
    relay_weights(wb, HD)
    relay_rows(far_half[0], True)
    arrive(near_half[0])
    relay_rows(far_half[1], False)
    arrive(near_half[1])
    for copy in relays[:2]:
        copy.wait_recv()
    hidden_far = hidden_rows(0, far_half)
    relay_rows(near_half[0], True)
    relay_rows(near_half[1], False)
    wait_weights(4, 5)
    relay_weights(db, NTP * HD // 2)
    relay_hidden(0, hidden_far)
    hidden_near = hidden_rows(1, near_half)
    for copy in relays[2:]:
        copy.wait_recv()
    give_back(0, far_half, hidden_far)
    relay_hidden(1, hidden_near)
    give_back(1, near_half, hidden_near)

    @pl.when(own_self)
    def _():
        rb[sp] = ob[0, c, y]

    for b in range(1, BACK + 1):

        @pl.when(sp + b < EXPERTS)
        def _():
            remote(pk, pk_in.at[b - 1], pk_s.at[b - 1], pk_r.at[b - 1], here).wait_send()

    @pl.when(sp + 1 < EXPERTS)
    def _():
        remote(edge, halo, halo_s, halo_r, here).wait_send()

    @pl.loop(1, NTP)
    def _(k):
        other = lax.rem(tp + k, NTP)
        remote(pg.at[tp], pg.at[tp], pg_s.at[other], pg_r.at[tp], here).wait_send()
        remote(st1.at[tp], st1.at[tp], st1_s.at[other], st1_r.at[tp], here).wait_send()

    @pl.loop(0, EXPERTS)
    def _(e):
        @pl.when(jnp.logical_not(jnp.logical_and(own_self, e == sp)))
        def _():
            remote(send_rows.at[e], rb.at[0], disp_s.at[e], disp_r.at[0, 0], here).wait_send()

    for pair in weights:
        relays.extend(pair)
    for copies in list(xf.values()) + [list(xr.values()), relays, hidden_far, hidden_near]:
        for copy in copies:
            copy.wait_send()

    @pl.loop(0, EXPERTS)
    def _(e):
        @pl.when(jnp.logical_not(jnp.logical_and(own_self, e == sp)))
        def _():
            remote(ob.at[0, 0, 0], rb.at[e], ret_s.at[0, 0], ret_r.at[e], here).wait_recv()

    picked = dot(pick[...], rb[...].reshape(EXPERTS * CAP, FD))
    moe = []
    for k in range(CHUNKS):
        both = [turned(rweight_ref[way : way + 1, k * LANE : (k + 1) * LANE]) for way in range(2)]
        moe.append(
            rows_of(picked, k) * both[0] + rows_of(picked, CHUNKS + k) * both[1]
        )
    final = ALPHA * nat[...] + jnp.concatenate(moe, axis=0)
    for k in range(CHUNKS):
        block = rows_of(final, k).T
        st2[tp, 0:1, k * LANE : (k + 1) * LANE] = jnp.sum(block, axis=0, keepdims=True)
        st2[tp, 1:2, k * LANE : (k + 1) * LANE] = jnp.sum(block * block, axis=0, keepdims=True)

    @pl.loop(1, NTP)
    def _(k):
        other = lax.rem(tp + k, NTP)
        remote(st2.at[tp], st2.at[tp], st2_s.at[other], st2_r.at[tp], plane_device(other)).start()

    @pl.loop(0, PIECES)
    def _(k):
        @pl.when(jnp.logical_not(jnp.logical_and(own_self, k == own_place)))
        def _():
            remote(
                ob.at[0, 0, 0],
                rb.at[0],
                ret_s.at[k // (NC * NY), lax.rem(k, NC * NY)],
                ret_r.at[0],
                here,
            ).wait_send()

    @pl.loop(1, NTP)
    def _(k):
        other = lax.rem(tp + k, NTP)
        remote(st2.at[tp], st2.at[other], st2_s.at[other], st2_r.at[other], here).wait_recv()

    mean, rstd = norm_columns(jnp.sum(st2[...], axis=0))
    for k in range(CHUNKS):
        centred = (rows_of(final, k) - turned(part(mean, k))) * turned(part(rstd, k))
        out_ref[k * LANE : (k + 1) * LANE, :] = (
            centred * gain2_ref[...] + bias2_ref[...]
        ).astype(BF16)

    @pl.loop(1, NTP)
    def _(k):
        other = lax.rem(tp + k, NTP)
        remote(st2.at[tp], st2.at[tp], st2_s.at[other], st2_r.at[tp], here).wait_send()


def body(
    pool_in,
    doc_ids,
    pool_map,
    pool_scale,
    w_out,
    gate_logit,
    residual,
    first_gain,
    first_bias,
    routes,
    route_weight,
    w_gate,
    w_up,
    w_down,
    second_gain,
    second_bias,
):
    vmem = pl.BlockSpec(memory_space=pltpu.VMEM)
    hbm = pl.BlockSpec(memory_space=pltpu.HBM)
    dma = pltpu.SemaphoreType.DMA
    args = (
        pool_in,
        doc_ids.reshape(CHUNKS, LANE),
        pool_map,
        pool_scale.reshape(1, -1),
        w_out,
        gate_logit,
        residual,
        first_gain.reshape(1, -1),
        first_bias.reshape(1, -1),
        routes.T,
        route_weight.T,
        w_gate[0].T,
        w_up[0].T,
        w_down[0],
        second_gain.reshape(1, -1),
        second_bias.reshape(1, -1),
    )
    in_specs = [hbm] * len(args)
    return pl.pallas_call(
        layer_kernel,
        out_shape=jax.ShapeDtypeStruct((TOK, FD), BF16),
        in_specs=in_specs,
        out_specs=vmem,
        scratch_shapes=[
            pltpu.VMEM((32, TOK), BF16),
            pltpu.VMEM((CHUNKS, LANE), jnp.int32),
            pltpu.VMEM((2 * NG, HD, HD), BF16),
            pltpu.VMEM((1, MIX_W), F32),
            pltpu.VMEM((MIX_W, FD), BF16),
            pltpu.VMEM((TOK, FD), BF16),
            pltpu.VMEM((TOK, FD), BF16),
            pltpu.VMEM((1, FD), F32),
            pltpu.VMEM((1, FD), F32),
            pltpu.VMEM((2, TOK), jnp.int32),
            pltpu.VMEM((2, TOK), F32),
            pltpu.VMEM((1, FD), F32),
            pltpu.VMEM((1, FD), F32),
            pltpu.VMEM((32, LANE), BF16),
            pltpu.VMEM((8, LANE), F32),
            pltpu.VMEM((BACK, 8, LANE), F32),
            pltpu.VMEM((NTP, 32, TOK), BF16),
            pltpu.VMEM((NTP, 2, TOK), F32),
            pltpu.VMEM((NTP, 2, TOK), F32),
            pltpu.VMEM((2, TOK), F32),
            pltpu.VMEM((EXPERTS, CAP, FD), BF16),
            pltpu.VMEM((NX, NG, NC, NY, CAP, FD), BF16),
            pltpu.VMEM((NY, 2 * HD, FEAT), BF16),
            pltpu.VMEM((NY, NTP * HD, FD), BF16),
            pltpu.VMEM((TOK // 2, NY * LANE), F32),
            pltpu.VMEM((NX, 2, TOK // 2, NY * HD), BF16),
            pltpu.VMEM((NG, NC, NY, CAP, FD), BF16),
            pltpu.VMEM((EXPERTS, CAP, FD), BF16),
            pltpu.VMEM((2 * TOK, EXPERTS * CAP), BF16),
            pltpu.VMEM((TOK, FD), F32),
            dma((len(args),)),
            pltpu.SemaphoreType.REGULAR,
            pltpu.SemaphoreType.REGULAR,
            dma,
            dma,
            dma((BACK,)),
            dma((BACK,)),
            dma((NTP,)),
            dma((NTP,)),
            dma((NTP,)),
            dma((NTP,)),
            dma((NTP,)),
            dma((NTP,)),
            dma((EXPERTS,)),
            dma((NG, NC * NY)),
            dma((3, NG)),
            dma((3, NG)),
            dma((16,)),
            dma((16,)),
            dma((2, 4)),
            dma((2, 4)),
            dma((NG, NC * NY)),
            dma((EXPERTS,)),
        ],
        compiler_params=pltpu.CompilerParams(
            collective_id=0, has_side_effects=True, vmem_limit_bytes=66_000_000
        ),
        cost_estimate=pl.CostEstimate(
            flops=2_000_000_000, bytes_accessed=4_000_000, transcendentals=0
        ),
        name="layer",
    )(*args)


def solution(mesh):
    finer = Mesh(mesh.devices.reshape(NZ, NC, NY, NX), ("z", "core", "y", "x"))
    sp = ("z", "core")
    in_specs = (
        P(TP, sp),
        P(sp),
        P(),
        P(),
        P(None, TP),
        P(sp, TP),
        P(sp, TP),
        P(TP),
        P(TP),
        P(sp, None),
        P(sp, None),
        P(sp, None, TP),
        P(sp, None, TP),
        P(sp, None, TP),
        P(TP),
        P(TP),
    )
    return jax.shard_map(
        body, mesh=finer, in_specs=in_specs, out_specs=P(sp, TP), check_vma=False
    )
```

time: 114 us -> 103 us (0.904)
  Pallas kernels: 108 us -> 101 us
  local copies, waits for them, and re-layouts: 5.02 us -> 1.54 us
    pallas_call x1, Pallas kernels: 108 us -> 101 us  [body(): pl.pallas_call(layer_kernel, out_shape=jax.ShapeDtypeStruct((TOK, FD), BF...]
    unnamed x31 -> x1, local copies, waits for them, and re-layouts: 4.29 us -> 1.54 us
where the time goes in v2:
time: 103 us
  Pallas kernels  101 us (98%)
  local copies, waits for them, and re-layouts  1.54 us (1%)
    pallas_call x1, Pallas kernels, body(): pl.pallas_call(layer_kernel, out_shape=jax.ShapeDtypeStruct((TOK, FD), BF...  101 us

profile of v2, /device:TPU:1, one launch (start us, length us, event | category | flops | bytes accessed | tf_op | source)
XLA Modules:
  0.0 102.7 jit_solution(11637201790209172610)
XLA Ops:
  0.0 101.1 %layer.1 = bf16[384,128]{1,0:T(8,128)(2,1)} custom-call(bf16[32,384]{1,0:T(8,128)(2,1)} %pool_h.1, s32[3,128]{1,0:T(4,128)} %bitcast.20, bf16[8,64,64]{2,1,0:T(8,128)(2,1)} %pmap_h.1, f32[1,512]{1,0:T(1,128)} %bitcast.21, bf16[512,128]{1,0:T(8,128)(2,1)} %wout_h.1, bf16[384,128]{1,0:T(8,128)(2,1)} %gate_h.1, bf16[384,128]{1,0:T(8,128)(2,1)} %res_h.1, ...), custom_call_target="tpu_custom_call" | custom-call | flops 2000000000 | bytes 4000000 | tf_op jit(solution)/shard_map/layer/pallas_call | solution.py:710
  101.1 1.5 %copy.18 = bf16[384,128]{1,0:T(8,128)(2,1)} copy(bf16[384,128]{1,0:T(8,128)(2,1)} %layer.1) | data formatting | bytes 196608

commit v3 on v2

--- a/solution.py
+++ b/solution.py
@@ -29,6 +29,12 @@
 NG = NZ // NY
 PIECES = NG * NC * NY
 ORDER = (2, 1, 3, 0)
+GROUP = NC * CAP
+STEPS = ("a2", "a1", "g2", "a3", "g1", "a0", "d2", "g3", "d1", "g0", "d3", "d0")
+HOPS = sorted(
+    ((dy, dx) for dy in range(NY) for dx in range(NX) if dy or dx),
+    key=lambda d: -min(d[0], NY - d[0]) - min(d[1], NX - d[1]),
+)
 
 
 def dot(a, b, dims=((1,), (0,))):
@@ -139,12 +145,16 @@
     here = (z, c, y, x)
     sp = z * NC + c
     tp = y * NX + x
-    right, left = lax.rem(x + 1, NX), lax.rem(x + NX - 1, NX)
-    across = lax.rem(x + 2, NX)
-    down, up = lax.rem(y + 1, NY), lax.rem(y + NY - 1, NY)
-    near = lax.rem(y - 2 * z + 2 * NZ, NY)
+    a = jnp.where(c == 0, y, x)
+    b = jnp.where(c == 0, x, y)
+    a_step = jnp.where(c == 0, NX, 1)
+    b_step = jnp.where(c == 0, 1, NX)
+    right, left = lax.rem(b + 1, NX), lax.rem(b + NX - 1, NX)
+    across = lax.rem(b + 2, NX)
+    down, up = lax.rem(a + 1, NY), lax.rem(a + NY - 1, NY)
+    near = lax.rem(a - 2 * z + 2 * NZ, NY)
     own_self = near == 0
-    own_place = c * NY + y
+    own_place = c * NY + a
 
     def sp_device(k):
         return (k // NC, lax.rem(k, NC), y, x)
@@ -152,21 +162,49 @@
     def plane_device(k):
         return (z, c, k // NX, lax.rem(k, NX))
 
+    def to_plane(buffer, send, recv):
+        for dy, dx in HOPS:
+            yy, xx = lax.rem(y + dy, NY), lax.rem(x + dx, NX)
+            other = yy * NX + xx
+            remote(
+                buffer.at[tp], buffer.at[tp], send.at[other], recv.at[tp], (z, c, yy, xx)
+            ).start()
+
     def line_device(dz):
         return (lax.rem(z + dz + NZ, NZ), c, y, x)
 
-    def expert_device(e):
-        ze = e // NC
-        return (ze, lax.rem(e, NC), lax.rem(z + ze, NY), x)
+    def turned_device(zz, cc, aa, bb):
+        first = cc == 0
+        return (zz, cc, jnp.where(first, aa, bb), jnp.where(first, bb, aa))
+
+    def expert_device(r):
+        ze = (z - r // NC) & (NZ - 1)
+        row = (z + ze) & (NY - 1)
+        return (ze, 0, row, x) if r % NC == 0 else (ze, 1, y, row)
+
+    def unless(mine, act):
+        if mine is None:
+            act()
+        else:
+            pl.when(jnp.logical_not(mine))(lambda: act())
+
+    def is_mine(q, k):
+        return jnp.logical_and(own_self, own_place == k) if q == 0 else None
 
     def source_device(q, k):
-        return (lax.rem(z + near + NY * q, NZ), k // NY, lax.rem(k, NY), x)
-
-    def neighbour(yy):
-        return (z, c, yy, x)
-
-    def beside(xx):
-        return (z, c, y, xx)
+        other = k % NY
+        return (
+            (z + near + NY * q) & (NZ - 1),
+            k // NY,
+            jnp.where(c == 0, other, b),
+            jnp.where(c == 0, b, other),
+        )
+
+    def neighbour(aa):
+        return turned_device(z, c, aa, b)
+
+    def beside(bb):
+        return turned_device(z, c, a, bb)
 
     def signal(sem, device):
         pl.semaphore_signal(sem, inc=1, device_id=device, device_id_type=MESH)
@@ -178,8 +216,8 @@
                 (pool_h, pool_ref),
                 (ids_h, ids_ref),
                 (routes_h, routes_ref),
-                (wg_h, wb.at[y, pl.ds(0, HD)]),
-                (wu_h, wb.at[y, pl.ds(HD, HD)]),
+                (wg_h, wb.at[a, pl.ds(0, HD)]),
+                (wu_h, wb.at[a, pl.ds(HD, HD)]),
                 (wout_h, wout_ref),
                 (gate_h, gate_ref),
                 (res_h, res_ref),
@@ -187,7 +225,7 @@
                 (scale_h, scale_ref),
                 (gain1_h, gain1_ref),
                 (bias1_h, bias1_ref),
-                (wd_h, db.at[y]),
+                (wd_h, db.at[a]),
                 (rweight_h, rweight_ref),
                 (gain2_h, gain2_ref),
                 (bias2_h, bias2_ref),
@@ -236,12 +274,16 @@
 
     pl.semaphore_wait(barrier, NTP - 1 + 5 * NC - 1)
 
-    for b in range(1, BACK + 1):
-
-        @pl.when(sp + b < EXPERTS)
+    for back in range(1, BACK + 1):
+
+        @pl.when(sp + back < EXPERTS)
         def _():
             remote(
-                pk, pk_in.at[b - 1], pk_s.at[b - 1], pk_r.at[b - 1], sp_device(sp + b)
+                pk,
+                pk_in.at[back - 1],
+                pk_s.at[back - 1],
+                pk_r.at[back - 1],
+                sp_device(sp + back),
             ).start()
 
     edge = pool_ref.at[:, pl.ds(TOK - LANE, LANE)]
@@ -257,7 +299,7 @@
 
     def send_weights(source, first, count):
         k = 2 * len(weights)
-        block = source.at[y, pl.ds(first, count)]
+        block = source.at[a, pl.ds(first, count)]
         pair = [
             remote(block, block, w_s.at[k], w_r.at[k], neighbour(down)),
             remote(block, block, w_s.at[k + 1], w_r.at[k + 1], neighbour(up)),
@@ -268,7 +310,7 @@
 
     loads[3].wait()
     loads[4].wait()
-    send_weights(wb, 0, 32)
+    send_weights(wb, 0, 64)
 
     for k in (2, *range(5, len(loads))):
         loads[k].wait()
@@ -296,17 +338,19 @@
     def _():
         remote(edge, halo, halo_s, halo_r, here).wait_recv()
 
-    for b in range(1, BACK + 1):
-
-        @pl.when(sp >= b)
+    for back in range(1, BACK + 1):
+
+        @pl.when(sp >= back)
         def _():
-            remote(pk, pk_in.at[b - 1], pk_s.at[b - 1], pk_r.at[b - 1], here).wait_recv()
+            remote(
+                pk, pk_in.at[back - 1], pk_s.at[back - 1], pk_r.at[back - 1], here
+            ).wait_recv()
 
     first_id = jnp.broadcast_to(ids[0][:, 0:1], (1, LANE))
     carry = jnp.zeros((1, LANE), F32)
-    for b in range(1, BACK + 1):
-        found = pk_in[b - 1]
-        same = (found[1:2] == first_id) & (jnp.broadcast_to(sp, (1, LANE)) >= b)
+    for back in range(1, BACK + 1):
+        found = pk_in[back - 1]
+        same = (found[1:2] == first_id) & (jnp.broadcast_to(sp, (1, LANE)) >= back)
         carry = carry + jnp.where(same, found[0:1], 0.0)
     carry_col = turned(carry)
     doc_flag = is_doc.astype(F32)
@@ -328,18 +372,17 @@
         pooled = total / count - part(pool, k).astype(F32)
         pg[tp, :, k * LANE : (k + 1) * LANE] = pooled.astype(BF16)
 
-    @pl.loop(1, NTP)
-    def _(k):
-        other = lax.rem(tp + k, NTP)
-        remote(pg.at[tp], pg.at[tp], pg_s.at[other], pg_r.at[tp], plane_device(other)).start()
-
-    send_weights(wb, 32, 16)
+    to_plane(pg, pg_s, pg_r)
+
+    send_weights(wb, 64, 16)
     pl.semaphore_wait(near_sem, 2)
     signal(far_sem, line_device(4))
     signal(far_sem, line_device(-4))
 
     expert = iota((EXPERTS, TOK), 0).astype(F32)
-    ways = [(expert == routes_ref[k : k + 1, :].astype(F32)).astype(F32) for k in range(2)]
+    routes = routes_ref[...]
+    routes = ((z - routes // NC) & (NZ - 1)) * NC + (routes & (NC - 1))
+    ways = [(expert == routes[k : k + 1].astype(F32)).astype(F32) for k in range(2)]
     earlier = (iota((TOK, TOK), 0) < iota((TOK, TOK), 1)).astype(F32).astype(BF16)
     rank = dot((ways[0] + ways[1]).astype(BF16), earlier) + expert * CAP
     for k in range(2):
@@ -361,12 +404,10 @@
 
     pl.semaphore_wait(far_sem, 2)
 
-    @pl.loop(1, NTP)
-    def _(k):
-        other = lax.rem(tp + k, NTP)
-        remote(st1.at[tp], st1.at[tp], st1_s.at[other], st1_r.at[tp], plane_device(other)).start()
-
-    send_weights(wb, 48, 64)
+    to_plane(st1, st1_s, st1_r)
+
+    send_weights(wb, 80, 48)
+    send_weights(db, 0, NTP * HD)
 
     @pl.loop(1, NTP)
     def _(k):
@@ -379,36 +420,29 @@
         [part(centred, k) * gain1 + bias1 for k in range(CHUNKS)], axis=1
     ).astype(BF16)
 
-    for k in range(8):
-        first = k * (EXPERTS * CAP // 8)
-        place = (iota((EXPERTS * CAP // 8, TOK), 0) + first).astype(F32)
+    span = NG * NC
+    for q in ORDER:
+        place = (iota((span * CAP, TOK), 0) + q * span * CAP).astype(F32)
         chosen = (place == slots[0:1, :]) | (place == slots[1:2, :])
         rows = dot(chosen.astype(F32).astype(BF16), normed, ((1,), (1,)))
-        send_rows[4 * k : 4 * k + 4] = rows.astype(BF16).reshape(4, CAP, FD)
-
-    for q in ORDER:
-
-        @pl.loop(0, NY * NC)
-        def _(k):
-            ze = lax.rem(z - k // NC - NY * q + 2 * NZ, NZ)
-            e = ze * NC + lax.rem(k, NC)
-
-            @pl.when(jnp.logical_not(jnp.logical_and(own_self, e == sp)))
-            def _():
+        send_rows[span * q : span * (q + 1)] = rows.astype(BF16).reshape(span, CAP, FD)
+
+        for r in range(span * q, span * (q + 1)):
+            row, column = (y, x) if r % NC == 0 else (x, y)
+            unless(
+                jnp.logical_and(own_self, c == r) if r < NC else None,
                 remote(
-                    send_rows.at[e],
-                    xb.at[x, q, c, y],
-                    disp_s.at[e],
-                    disp_r.at[q, own_place],
-                    expert_device(e),
-                ).start()
+                    send_rows.at[r],
+                    xb.at[column, q, c, row],
+                    disp_s.at[r],
+                    disp_r.at[q, c * NY + row],
+                    expert_device(r),
+                ).start,
+            )
 
     @pl.when(own_self)
     def _():
-        xb[x, 0, c, y] = send_rows[sp]
-
-    send_weights(wb, 112, 16)
-    send_weights(db, 0, NTP * HD)
+        xb[b, 0, c, a] = send_rows[c]
 
     for k in range(CHUNKS):
         nat[k * LANE : (k + 1) * LANE] = part(normed, k).astype(F32).T
@@ -423,7 +457,7 @@
     relays = []
 
     def relay_weights(source, count):
-        k = 2 * len(weights) + len(relays)
+        k = 8 + len(relays)
         from_up = source.at[up, pl.ds(0, count)]
         from_down = source.at[down, pl.ds(count, count)]
         pair = [
@@ -439,157 +473,143 @@
             for copy in pair:
                 copy.wait_recv()
 
-    xf, xr = {}, {}
+    wait_weights(0, 4)
+    relay_weights(wb, HD)
+    relay_weights(db, NTP * HD // 2)
+
+    xf = {}
 
     def arrive(q):
-        @pl.loop(0, NC * NY)
-        def _(k):
-            mine = jnp.logical_and(own_self, k == own_place) if q == 0 else jnp.bool_(False)
-
-            @pl.when(jnp.logical_not(mine))
-            def _():
+        for k in range(NC * NY):
+            unless(
+                is_mine(q, k),
                 remote(
                     send_rows.at[0],
-                    xb.at[x, q, k // NY, lax.rem(k, NY)],
+                    xb.at[b, q, k // NY, k % NY],
                     disp_s.at[0],
                     disp_r.at[q, k],
                     here,
-                ).wait_recv()
-
-        mine = xb.at[x, q]
+                ).wait_recv,
+            )
+
+        mine = xb.at[b, q]
         xf[q] = [
             remote(mine, mine, xf_s.at[0, q], xf_r.at[0, q], beside(right)),
             remote(mine, mine, xf_s.at[1, q], xf_r.at[1, q], beside(left)),
+            remote(mine, mine, xf_s.at[2, q], xf_r.at[2, q], beside(across)),
         ]
         for copy in xf[q]:
             copy.start()
 
-    def relay_rows(q, to_right):
-        for copy in xf[q]:
-            copy.wait_recv()
-        piece = xb.at[left if to_right else right, q]
-        xr[q] = remote(
-            piece, piece, xf_s.at[2, q], xf_r.at[2, q], beside(right if to_right else left)
-        )
-        xr[q].start()
-
-    def projected(pair, xx):
-        tiles, columns = [], []
-        for yy in range(NY):
-            block = [xb[xx, q, :, yy].reshape(NC * CAP, FD) for q in pair]
-            tiles.append(jnp.concatenate(block, axis=0))
-            start = pl.multiple_of((yy * NX + xx) * FD, FD)
+    def projected(group, bb):
+        tiles = [
+            jnp.concatenate([xb[bb, q, :, aa].reshape(GROUP, FD) for q in group], axis=0)
+            for aa in range(NY)
+        ]
+        columns = []
+        for aa in range(NY):
+            start = pl.multiple_of((aa * a_step + bb * b_step) * FD, FD)
             columns.append(
-                jnp.concatenate([wb[b, :, pl.ds(start, FD)] for b in range(NY)], axis=0)
+                jnp.concatenate([wb[k, :, pl.ds(start, FD)] for k in range(NY)], axis=0)
             )
         return dot(
             jnp.concatenate(tiles, axis=1), jnp.concatenate(columns, axis=1), ((1,), (1,))
         )
 
-    half = TOK // 2
-    low = iota((half, LANE), 1) < HD
-
-    def hidden_rows(number, pair):
-        for q in pair:
-            xr[q].wait_recv()
-        acc[...] = projected(pair, x)
-        for xx in (left, right, across):
-            acc[...] += projected(pair, xx)
+    hx = {}
+
+    def hidden_rows(group):
+        size = len(group) * GROUP
+        low = iota((size, LANE), 1) < HD
+        acc[:size] = projected(group, b)
+        for number, bb in enumerate((left, right, across)):
+            for q in group:
+                xf[q][number].wait_recv()
+            acc[:size] += projected(group, bb)
         for k in range(NY // 2):
-            one = acc[:, 2 * k * LANE : (2 * k + 1) * LANE]
-            two = acc[:, (2 * k + 1) * LANE : (2 * k + 2) * LANE]
+            one = acc[:size, 2 * k * LANE : (2 * k + 1) * LANE]
+            two = acc[:size, (2 * k + 1) * LANE : (2 * k + 2) * LANE]
             gate = jnp.where(low, one, pltpu.roll(two, HD, 1))
             lift = jnp.where(low, pltpu.roll(one, HD, 1), two)
-            hidden = gate * jax.nn.sigmoid(gate) * lift
-            hb[x, number, :, k * LANE : (k + 1) * LANE] = hidden.astype(BF16)
-        mine = hb.at[x, number]
-        copies = [
-            remote(mine, mine, h_s.at[number, 0], h_r.at[number, 0], beside(right)),
-            remote(mine, mine, h_s.at[number, 1], h_r.at[number, 1], beside(left)),
+            hidden = (gate * jax.nn.sigmoid(gate) * lift).astype(BF16)
+            for number, q in enumerate(group):
+                hb[b, q, :, k * LANE : (k + 1) * LANE] = hidden[
+                    number * GROUP : (number + 1) * GROUP
+                ]
+        for q in group:
+            mine = hb.at[b, q]
+            hx[q] = [
+                remote(mine, mine, h_s.at[q, k], h_r.at[q, k], beside(bb))
+                for k, bb in enumerate((right, left, across))
+            ]
+            for copy in hx[q]:
+                copy.start()
+
+    def lowered(group, bb):
+        starts = [
+            pl.multiple_of((aa * a_step + bb * b_step) * HD, HD) for aa in range(NY)
         ]
-        for copy in copies:
-            copy.start()
-        return copies
-
-    def relay_hidden(number, copies):
-        copies[0].wait_recv()
-        piece = hb.at[left, number, pl.ds(0, half // 2)]
-        first = remote(piece, piece, h_s.at[number, 2], h_r.at[number, 2], beside(right))
-        first.start()
-        copies[1].wait_recv()
-        piece = hb.at[right, number, pl.ds(half // 2, half // 2)]
-        second = remote(piece, piece, h_s.at[number, 3], h_r.at[number, 3], beside(left))
-        second.start()
-        copies += [first, second]
-
-    def lowered(number, xx):
-        blocks = []
-        for yy in range(NY):
-            pieces = [
-                db[yy, pl.ds(pl.multiple_of((b * NX + xx) * HD, HD), HD), :] for b in range(NY)
-            ]
-            blocks.append(jnp.concatenate(pieces, axis=0))
-        return dot(hb[xx, number], jnp.concatenate(blocks, axis=1))
-
-    def give_back(number, pair, copies):
-        acc[...] = lowered(number, x)
-        acc[...] += lowered(number, left)
-        acc[...] += lowered(number, right)
-        copies[2].wait_recv()
-        copies[3].wait_recv()
-        result = (acc[...] + lowered(number, across)).astype(BF16)
-        for k, q in enumerate(pair):
-            rows = result[k * NC * CAP : (k + 1) * NC * CAP]
-            for yy in range(NY):
-                ob[q, :, yy] = part(rows, yy).reshape(NC, CAP, FD)
-
-            @pl.loop(0, NC * NY)
-            def _(k):
-                mine = jnp.logical_and(own_self, k == own_place) if q == 0 else jnp.bool_(False)
-
-                @pl.when(jnp.logical_not(mine))
-                def _():
+        blocks = [
+            jnp.concatenate([db[k, pl.ds(start, HD), :] for start in starts], axis=0)
+            for k in range(NY)
+        ]
+        rows = jnp.concatenate([hb[bb, q] for q in group], axis=0)
+        return dot(rows, jnp.concatenate(blocks, axis=1))
+
+    def give_back(group):
+        size = len(group) * GROUP
+        acc[:size] = lowered(group, b)
+        for number, bb in enumerate((left, right, across)):
+            for q in group:
+                hx[q][number].wait_recv()
+            acc[:size] += lowered(group, bb)
+        result = acc[:size].astype(BF16)
+        for number, q in enumerate(group):
+            rows = result[number * GROUP : (number + 1) * GROUP]
+            for aa in range(NY):
+                ob[q, :, aa] = part(rows, aa).reshape(NC, CAP, FD)
+            place = q * NG * NC + near * NC + c
+            for k in range(NC * NY):
+                unless(
+                    is_mine(q, k),
                     remote(
-                        ob.at[q, k // NY, lax.rem(k, NY)],
-                        rb.at[sp],
+                        ob.at[q, k // NY, k % NY],
+                        rb.at[place],
                         ret_s.at[q, k],
-                        ret_r.at[sp],
+                        ret_r.at[place],
                         source_device(q, k),
-                    ).start()
-
-    far_half, near_half = ORDER[:2], ORDER[2:]
-    arrive(far_half[0])
-    arrive(far_half[1])
-    wait_weights(0, 4)
-    relay_weights(wb, HD)
-    relay_rows(far_half[0], True)
-    arrive(near_half[0])
-    relay_rows(far_half[1], False)
-    arrive(near_half[1])
-    for copy in relays[:2]:
-        copy.wait_recv()
-    hidden_far = hidden_rows(0, far_half)
-    relay_rows(near_half[0], True)
-    relay_rows(near_half[1], False)
-    wait_weights(4, 5)
-    relay_weights(db, NTP * HD // 2)
-    relay_hidden(0, hidden_far)
-    hidden_near = hidden_rows(1, near_half)
-    for copy in relays[2:]:
-        copy.wait_recv()
-    give_back(0, far_half, hidden_far)
-    relay_hidden(1, hidden_near)
-    give_back(1, near_half, hidden_near)
+                    ).start,
+                )
+
+    first_hidden, first_down = True, True
+    for step in STEPS:
+        group = [int(q) for q in step[1:]]
+        if step[0] == "a":
+            arrive(group[0])
+        elif step[0] == "g":
+            if first_hidden:
+                for copy in relays[:2]:
+                    copy.wait_recv()
+            first_hidden = False
+            hidden_rows(group)
+        else:
+            if first_down:
+                for copy in relays[2:]:
+                    copy.wait_recv()
+            first_down = False
+            give_back(group)
 
     @pl.when(own_self)
     def _():
-        rb[sp] = ob[0, c, y]
-
-    for b in range(1, BACK + 1):
-
-        @pl.when(sp + b < EXPERTS)
+        rb[c] = ob[0, c, a]
+
+    for back in range(1, BACK + 1):
+
+        @pl.when(sp + back < EXPERTS)
         def _():
-            remote(pk, pk_in.at[b - 1], pk_s.at[b - 1], pk_r.at[b - 1], here).wait_send()
+            remote(
+                pk, pk_in.at[back - 1], pk_s.at[back - 1], pk_r.at[back - 1], here
+            ).wait_send()
 
     @pl.when(sp + 1 < EXPERTS)
     def _():
@@ -603,23 +623,28 @@
 
     @pl.loop(0, EXPERTS)
     def _(e):
-        @pl.when(jnp.logical_not(jnp.logical_and(own_self, e == sp)))
+        @pl.when(jnp.logical_not(jnp.logical_and(own_self, e == c)))
         def _():
             remote(send_rows.at[e], rb.at[0], disp_s.at[e], disp_r.at[0, 0], here).wait_send()
 
-    for pair in weights:
-        relays.extend(pair)
-    for copies in list(xf.values()) + [list(xr.values()), relays, hidden_far, hidden_near]:
+    for copies in weights + list(xf.values()) + list(hx.values()) + [relays]:
         for copy in copies:
             copy.wait_send()
 
-    @pl.loop(0, EXPERTS)
-    def _(e):
-        @pl.when(jnp.logical_not(jnp.logical_and(own_self, e == sp)))
-        def _():
-            remote(ob.at[0, 0, 0], rb.at[e], ret_s.at[0, 0], ret_r.at[e], here).wait_recv()
-
-    picked = dot(pick[...], rb[...].reshape(EXPERTS * CAP, FD))
+    picked = None
+    for q in ORDER:
+        for r in range(NG * NC * q, NG * NC * (q + 1)):
+            unless(
+                jnp.logical_and(own_self, c == r) if r < NC else None,
+                remote(ob.at[0, 0, 0], rb.at[r], ret_s.at[0, 0], ret_r.at[r], here).wait_recv,
+            )
+
+        group = NG * NC * CAP
+        rows = dot(
+            pick[:, q * group : (q + 1) * group],
+            rb[NG * NC * q : NG * NC * (q + 1)].reshape(group, FD),
+        )
+        picked = rows if picked is None else picked + rows
     moe = []
     for k in range(CHUNKS):
         both = [turned(rweight_ref[way : way + 1, k * LANE : (k + 1) * LANE]) for way in range(2)]
@@ -632,10 +657,7 @@
         st2[tp, 0:1, k * LANE : (k + 1) * LANE] = jnp.sum(block, axis=0, keepdims=True)
         st2[tp, 1:2, k * LANE : (k + 1) * LANE] = jnp.sum(block * block, axis=0, keepdims=True)
 
-    @pl.loop(1, NTP)
-    def _(k):
-        other = lax.rem(tp + k, NTP)
-        remote(st2.at[tp], st2.at[tp], st2_s.at[other], st2_r.at[tp], plane_device(other)).start()
+    to_plane(st2, st2_s, st2_r)
 
     @pl.loop(0, PIECES)
     def _(k):
@@ -737,8 +759,8 @@
             pltpu.VMEM((NX, NG, NC, NY, CAP, FD), BF16),
             pltpu.VMEM((NY, 2 * HD, FEAT), BF16),
             pltpu.VMEM((NY, NTP * HD, FD), BF16),
-            pltpu.VMEM((TOK // 2, NY * LANE), F32),
-            pltpu.VMEM((NX, 2, TOK // 2, NY * HD), BF16),
+            pltpu.VMEM((TOK, NY * LANE), F32),
+            pltpu.VMEM((NX, NG, GROUP, NY * HD), BF16),
             pltpu.VMEM((NG, NC, NY, CAP, FD), BF16),
             pltpu.VMEM((EXPERTS, CAP, FD), BF16),
             pltpu.VMEM((2 * TOK, EXPERTS * CAP), BF16),
@@ -762,8 +784,8 @@
             dma((3, NG)),
             dma((16,)),
             dma((16,)),
-            dma((2, 4)),
-            dma((2, 4)),
+            dma((NG, 3)),
+            dma((NG, 3)),
             dma((NG, NC * NY)),
             dma((EXPERTS,)),
         ],

time: 103 us -> 87.8 us (0.85)
  Pallas kernels: 101 us -> 86.1 us
    pallas_call x1, Pallas kernels: 101 us -> 86.1 us  [body(): pl.pallas_call(layer_kernel, out_shape=jax.ShapeDtypeStruct((TOK, FD), BF...]
where the time goes in v3:
time: 87.8 us; the launch traced here: 87.6 us
  Pallas kernels  86.1 us (98%)
  local copies, waits for them, and re-layouts  1.54 us (2%)
    pallas_call x1, Pallas kernels, body(): pl.pallas_call(layer_kernel, out_shape=jax.ShapeDtypeStruct((TOK, FD), BF...  86.1 us

profile of v3, /device:TPU:1, one launch (start us, length us, event | category | flops | bytes accessed | tf_op | source)
XLA Modules:
  0.0 87.6 jit_solution(11402852969834481675)
XLA Ops:
  0.0 86.1 %layer.1 = bf16[384,128]{1,0:T(8,128)(2,1)} custom-call(bf16[32,384]{1,0:T(8,128)(2,1)} %pool_h.1, s32[3,128]{1,0:T(4,128)} %bitcast.20, bf16[8,64,64]{2,1,0:T(8,128)(2,1)} %pmap_h.1, f32[1,512]{1,0:T(1,128)} %bitcast.21, bf16[512,128]{1,0:T(8,128)(2,1)} %wout_h.1, bf16[384,128]{1,0:T(8,128)(2,1)} %gate_h.1, bf16[384,128]{1,0:T(8,128)(2,1)} %res_h.1, ...), custom_call_target="tpu_custom_call" | custom-call | flops 2000000000 | bytes 4000000 | tf_op jit(solution)/shard_map/layer/pallas_call | solution.py:732
  86.1 1.5 %copy.18 = bf16[384,128]{1,0:T(8,128)(2,1)} copy(bf16[384,128]{1,0:T(8,128)(2,1)} %layer.1) | data formatting | bytes 196608

commit v4 on v3

--- a/solution.py
+++ b/solution.py
@@ -116,6 +116,7 @@
     ob,
     rb,
     pick,
+    chosen,
     nat,
     load_sem,
     near_sem,
@@ -310,7 +311,7 @@
 
     loads[3].wait()
     loads[4].wait()
-    send_weights(wb, 0, 64)
+    send_weights(wb, 0, 32)
 
     for k in (2, *range(5, len(loads))):
         loads[k].wait()
@@ -374,7 +375,7 @@
 
     to_plane(pg, pg_s, pg_r)
 
-    send_weights(wb, 64, 16)
+    send_weights(wb, 32, 16)
     pl.semaphore_wait(near_sem, 2)
     signal(far_sem, line_device(4))
     signal(far_sem, line_device(-4))
@@ -387,6 +388,11 @@
     rank = dot((ways[0] + ways[1]).astype(BF16), earlier) + expert * CAP
     for k in range(2):
         slots[k : k + 1, :] = jnp.sum(ways[k] * rank, axis=0, keepdims=True)
+    span = NG * NC
+    for q in range(NG):
+        place = (iota((span * CAP, TOK), 0) + q * span * CAP).astype(F32)
+        wanted = (place == slots[0:1, :]) | (place == slots[1:2, :])
+        chosen[q] = wanted.astype(F32).astype(BF16)
 
     @pl.loop(1, NTP)
     def _(k):
@@ -406,7 +412,7 @@
 
     to_plane(st1, st1_s, st1_r)
 
-    send_weights(wb, 80, 48)
+    send_weights(wb, 48, 80)
     send_weights(db, 0, NTP * HD)
 
     @pl.loop(1, NTP)
@@ -420,11 +426,8 @@
         [part(centred, k) * gain1 + bias1 for k in range(CHUNKS)], axis=1
     ).astype(BF16)
 
-    span = NG * NC
     for q in ORDER:
-        place = (iota((span * CAP, TOK), 0) + q * span * CAP).astype(F32)
-        chosen = (place == slots[0:1, :]) | (place == slots[1:2, :])
-        rows = dot(chosen.astype(F32).astype(BF16), normed, ((1,), (1,)))
+        rows = dot(chosen[q], normed, ((1,), (1,)))
         send_rows[span * q : span * (q + 1)] = rows.astype(BF16).reshape(span, CAP, FD)
 
         for r in range(span * q, span * (q + 1)):
@@ -764,6 +767,7 @@
             pltpu.VMEM((NG, NC, NY, CAP, FD), BF16),
             pltpu.VMEM((EXPERTS, CAP, FD), BF16),
             pltpu.VMEM((2 * TOK, EXPERTS * CAP), BF16),
+            pltpu.VMEM((NG, EXPERTS * CAP // NG, TOK), BF16),
             pltpu.VMEM((TOK, FD), F32),
             dma((len(args),)),
             pltpu.SemaphoreType.REGULAR,

time: 87.8 us -> 86.8 us (0.989)
  Pallas kernels: 86.1 us -> 85.1 us
    pallas_call x1, Pallas kernels: 86.1 us -> 85.1 us  [body(): pl.pallas_call(layer_kernel, out_shape=jax.ShapeDtypeStruct((TOK, FD), BF...]
where the time goes in v4:
time: 86.8 us; the launch traced here: 86.7 us
  Pallas kernels  85.1 us (98%)
  local copies, waits for them, and re-layouts  1.54 us (2%)
    pallas_call x1, Pallas kernels, body(): pl.pallas_call(layer_kernel, out_shape=jax.ShapeDtypeStruct((TOK, FD), BF...  85.1 us

profile of v4, /device:TPU:1, one launch (start us, length us, event | category | flops | bytes accessed | tf_op | source)
XLA Modules:
  0.0 86.7 jit_solution(13073874634400507734)
XLA Ops:
  0.0 85.1 %layer.1 = bf16[384,128]{1,0:T(8,128)(2,1)} custom-call(bf16[32,384]{1,0:T(8,128)(2,1)} %pool_h.1, s32[3,128]{1,0:T(4,128)} %bitcast.20, bf16[8,64,64]{2,1,0:T(8,128)(2,1)} %pmap_h.1, f32[1,512]{1,0:T(1,128)} %bitcast.21, bf16[512,128]{1,0:T(8,128)(2,1)} %wout_h.1, bf16[384,128]{1,0:T(8,128)(2,1)} %gate_h.1, bf16[384,128]{1,0:T(8,128)(2,1)} %res_h.1, ...), custom_call_target="tpu_custom_call" | custom-call | flops 2000000000 | bytes 4000000 | tf_op jit(solution)/shard_map/layer/pallas_call | solution.py:735
  85.1 1.5 %copy.18 = bf16[384,128]{1,0:T(8,128)(2,1)} copy(bf16[384,128]{1,0:T(8,128)(2,1)} %layer.1) | data formatting | bytes 196608

commit v5 on v4

--- a/solution.py
+++ b/solution.py
@@ -233,8 +233,6 @@
             ]
         )
     ]
-    for load in loads:
-        load.start()
     barrier = pltpu.get_barrier_semaphore()
     for dz in range(-2, 3):
         for other in range(NC):
@@ -245,6 +243,9 @@
     @pl.loop(1, NTP)
     def _(k):
         signal(barrier, plane_device(lax.rem(tp + k, NTP)))
+
+    for load in loads:
+        load.start()
 
     loads[0].wait()
     loads[1].wait()

time: 86.8 us -> 86.8 us (level)
  no operation moved by 1% of the time
where the time goes in v5:
time: 86.8 us; the launch traced here: 86.7 us
  Pallas kernels  85.1 us (98%)
  local copies, waits for them, and re-layouts  1.54 us (2%)
    pallas_call x1, Pallas kernels, body(): pl.pallas_call(layer_kernel, out_shape=jax.ShapeDtypeStruct((TOK, FD), BF...  85.1 us

profile of v5, /device:TPU:1, one launch (start us, length us, event | category | flops | bytes accessed | tf_op | source)
XLA Modules:
  0.0 86.7 jit_solution(3375938153368063304)
XLA Ops:
  0.0 85.1 %layer.1 = bf16[384,128]{1,0:T(8,128)(2,1)} custom-call(bf16[32,384]{1,0:T(8,128)(2,1)} %pool_h.1, s32[3,128]{1,0:T(4,128)} %bitcast.20, bf16[8,64,64]{2,1,0:T(8,128)(2,1)} %pmap_h.1, f32[1,512]{1,0:T(1,128)} %bitcast.21, bf16[512,128]{1,0:T(8,128)(2,1)} %wout_h.1, bf16[384,128]{1,0:T(8,128)(2,1)} %gate_h.1, bf16[384,128]{1,0:T(8,128)(2,1)} %res_h.1, ...), custom_call_target="tpu_custom_call" | custom-call | flops 2000000000 | bytes 4000000 | tf_op jit(solution)/shard_map/layer/pallas_call | solution.py:736
  85.1 1.5 %copy.18 = bf16[384,128]{1,0:T(8,128)(2,1)} copy(bf16[384,128]{1,0:T(8,128)(2,1)} %layer.1) | data formatting | bytes 196608
